TPU v7x, 32 devices: a whole 2x2x4 slice. The times are simulated.
32 devices in a mesh: ep: 8 (over z, core), tp: 4 (over y, x).
Axes of the slice: x: 2, y: 2, z: 4, core: 2. Of those that a mesh axis runs over, the one named last changes fastest.
Arguments:
- tokens: bfloat16 [4096, 2048], P(('ep', 'tp')), may hold values from -6 to 6
- norm_gain: float32 [2048], replicated, may hold values from 0.1 to 1.9
- expert_ids: int32 [4096, 2], P(('ep', 'tp')), may hold values from 0 to 7, all different within a row; in each aligned block of 128 rows (0 to 127, 128 to 255, ...) at most 64 rows name the same one
- gate_weights: float32 [4096, 2], P(('ep', 'tp')), may hold values from 0.2 to 1.6
- expert_gate: bfloat16 [8, 512, 2048], P('ep', 'tp'), may hold values from -0.125 to 0.125
- expert_up: bfloat16 [8, 512, 2048], P('ep', 'tp'), may hold values from -0.125 to 0.125
- expert_down: bfloat16 [8, 512, 2048], P('ep', 'tp'), may hold values from -0.25 to 0.25
- shared_gate: bfloat16 [512, 2048], P('tp'), may hold values from -0.125 to 0.125
- shared_up: bfloat16 [512, 2048], P('tp'), may hold values from -0.125 to 0.125
- shared_down: bfloat16 [512, 2048], P('tp'), may hold values from -0.25 to 0.25
Outputs:
- mixed: bfloat16 [4096, 2048], P(('ep', 'tp'))
Inputs may be any that keep to these rules, and one draw needn't show every extreme that they name: `expert_ids`: each row names 2 different experts. Within the rows of one device no expert is named by more than 64 rows, and in every draw some expert is named by exactly 64 rows of some device.
All inputs are finite; a program needn't handle non-finite values.
Results may differ from a plain program's by a relative error of at most 0.0068.
Values may be sent and summed in bfloat16 or wider, within the bound.
No kernel may reach another device: no remote copies, remote signals or barrier semaphores. Data moves between devices by JAX's collectives and lax.ppermute only.
A program may use at most 64 MiB of HBM per device.

v0:
```python
import jax
import jax.numpy as jnp
from jax import lax
from jax.sharding import PartitionSpec as P

EPS = 1e-06


def for_sending(shard):
    return jax.tree.map(lambda a: a.astype(jnp.bfloat16) if a.dtype == jnp.float32 else a, shard)


def against(rows, weight):
    return lax.dot_general(
        rows, weight, (((1,), (1,)), ((), ())), preferred_element_type=jnp.float32
    )


def hidden_block(rows, gate_rows, up_rows):
    return (jax.nn.silu(against(rows, gate_rows)) * against(rows, up_rows)).astype(jnp.bfloat16)


def apart_mlp(rows, gate, up, down, width, collect_pair, collect_rest):

    def fill_hidden(hidden, pieces, start):
        block = hidden_block(rows, pieces[0], pieces[1])
        return block

    hidden = collect_pair((gate, up), fill_hidden, jnp.zeros((rows.shape[0], width), jnp.bfloat16))

    def add_down(total, piece, start):
        return jnp.dot(hidden, piece, preferred_element_type=jnp.float32)

    empty = jnp.zeros((rows.shape[0], down.shape[1]), jnp.float32)
    return collect_rest(down, add_down, empty)


def body(
    tokens,
    norm_gain,
    expert_ids,
    gate_weights,
    expert_gate,
    expert_up,
    expert_down,
    shared_gate,
    shared_up,
    shared_down,
):
    tok = tokens.astype(jnp.float32)
    normed = (
        tok * lax.rsqrt(jnp.mean(tok * tok, axis=-1, keepdims=True) + EPS) * norm_gain
    ).astype(jnp.bfloat16)
    groups = lax.axis_size("tp")
    count = lax.axis_size("ep")
    tok_rows, chosen = expert_ids.shape
    features = tokens.shape[1]
    capacity = 2 * tok_rows * chosen // count
    labels = jnp.arange(count, dtype=jnp.int32)
    hits = jnp.sum((expert_ids[:, :, None] == labels[None, None, :]).astype(jnp.int32), axis=1)
    before = jnp.cumsum(hits, axis=0) - hits
    slot_of = jnp.take_along_axis(before, expert_ids, axis=1)
    flat_pos = expert_ids * capacity + slot_of
    slots = jnp.arange(count * capacity, dtype=jnp.int32)
    placing = jnp.any(flat_pos[:, :, None] == slots[None, None, :], axis=1).astype(jnp.bfloat16)
    outgoing = lax.dot_general(
        placing, normed, (((0,), (0,)), ((), ())), preferred_element_type=jnp.float32
    )
    outgoing = outgoing.astype(jnp.bfloat16).reshape(count, capacity, features)
    arrived = lax.all_to_all(outgoing, "ep", split_axis=0, concat_axis=0, tiled=True)
    rows = arrived.reshape(count * capacity, features)
    width = expert_gate.shape[1] * groups
    results = apart_mlp(
        rows,
        expert_gate[0],
        expert_up[0],
        expert_down[0],
        width,
        lambda x, fn, init: fn(
            init,
            jax.tree.map(lambda a: lax.all_gather(a, "tp", axis=0, tiled=True), for_sending(x)),
            jnp.int32(0),
        ),
        lambda x, fn, init: fn(init, lax.all_gather(x, "tp", axis=0, tiled=True), jnp.int32(0)),
    )
    results = results.astype(jnp.bfloat16).reshape(count, capacity, features)
    returned = lax.all_to_all(results, "ep", split_axis=0, concat_axis=0, tiled=True).reshape(
        count * capacity, features
    )
    picked = jnp.take(returned, flat_pos.reshape(-1), axis=0).reshape(tok_rows, chosen, features)
    routed = jnp.sum(gate_weights[:, :, None] * picked.astype(jnp.float32), axis=1)
    width = shared_gate.shape[0] * groups
    shared = apart_mlp(
        normed,
        shared_gate,
        shared_up,
        shared_down,
        width,
        lambda x, fn, init: fn(
            init,
            jax.tree.map(lambda a: lax.all_gather(a, "tp", axis=0, tiled=True), for_sending(x)),
            jnp.int32(0),
        ),
        lambda x, fn, init: fn(init, lax.all_gather(x, "tp", axis=0, tiled=True), jnp.int32(0)),
    )
    return (routed + shared).astype(jnp.bfloat16)


def solution(mesh):
    in_specs = (
        P(("ep", "tp"), None),
        P(),
        P(("ep", "tp"), None),
        P(("ep", "tp"), None),
        P("ep", "tp", None),
        P("ep", "tp", None),
        P("ep", "tp", None),
        P("tp", None),
        P("tp", None),
        P("tp", None),
    )
    out_specs = P(("ep", "tp"), None)
    return jax.shard_map(body, mesh=mesh, in_specs=in_specs, out_specs=out_specs, check_vma=False)
```

profile of v0, /device:TPU:0, one launch (start us, length us, event | category | flops | bytes accessed | tf_op | source)
XLA Modules:
  0.0 243.0 jit_solution(15632177701274800440)
XLA Ops:
  6.5 0.7 all-gather.16.cloned.1.call-update
  7.3 0.7 all-gather.18.cloned.1.call-update
  8.1 0.7 all-gather.20.cloned.1.call-update
  8.8 0.5 all-gather.10.cloned.1.call-update
  9.9 1.9 gather_fusion.1
  12.5 2.1 convolution_convert_fusion.1
  14.6 6.4 %all-to-all-start = ((bf16[8,64,2048]{2,1,0:T(8,128)(2,1)}), bf16[8,64,2048]{2,1,0:T(8,128)(2,1)S(1)}, u32[]{:S(2)}, u32[]{:S(2)}) async-start(bf16[8,64,2048]{2,1,0:T(8,128)(2,1)} %bitcast.1), calls=%async_computation | async-start | bytes 4194304 | tf_op jit(solution)/shard_map/all_to_all | solution.py:70
  21.0 0.5 all-gather.12.cloned.1.call-update
  21.5 25.6 %all-gather.16.cloned.1.call-done = bf16[1,512,2048]{2,1,0:T(8,128)(2,1)} async-done(((bf16[1,128,2048]{2,1,0:T(8,128)(2,1)}), bf16[1,512,2048]{2,1,0:T(8,128)(2,1)}) %all-gather.16.cloned.1.call-update) | async-done | bytes 2097168 | tf_op jit(solution)/shard_map/all_gather | solution.py:81
  47.1 22.9 %all-to-all-done = bf16[8,64,2048]{2,1,0:T(8,128)(2,1)S(1)} async-done(((bf16[8,64,2048]{2,1,0:T(8,128)(2,1)}), bf16[8,64,2048]{2,1,0:T(8,128)(2,1)S(1)}, u32[]{:S(2)}, u32[]{:S(2)}) %all-to-all-start) | async-done | bytes 2097184 | tf_op jit(solution)/shard_map/all_to_all | solution.py:70
  70.0 4.1 %fusion.4 = f32[512,512]{1,0:T(8,128)} fusion(bf16[512,2048]{1,0:T(8,128)(2,1)S(1)} %bitcast.32, bf16[1,512,2048]{2,1,0:T(8,128)(2,1)} %all-gather.16.cloned.1.call-done), kind=kOutput, calls=%fused_computation.9 | convolution fusion | flops 1073741824 | bytes 5242880 | tf_op jit(solution)/shard_map/dot_general | solution.py:14
  74.1 10.0 %all-gather.18.cloned.1.call-done = bf16[1,512,2048]{2,1,0:T(8,128)(2,1)} async-done(((bf16[1,128,2048]{2,1,0:T(8,128)(2,1)}), bf16[1,512,2048]{2,1,0:T(8,128)(2,1)}) %all-gather.18.cloned.1.call-update) | async-done | bytes 2097168 | tf_op jit(solution)/shard_map/all_gather | solution.py:81
  84.2 37.1 %all-gather.20.cloned.1.call-done = bf16[1,512,2048]{2,1,0:T(8,128)(2,1)} async-done(((bf16[1,128,2048]{2,1,0:T(8,128)(2,1)}), bf16[1,512,2048]{2,1,0:T(8,128)(2,1)}) %all-gather.20.cloned.1.call-update) | async-done | bytes 2097168 | tf_op jit(solution)/shard_map/all_gather | solution.py:84
  121.2 6.4 %convolution_convert_fusion = bf16[512,2048]{1,0:T(8,128)(2,1)} fusion(bf16[1,512,2048]{2,1,0:T(8,128)(2,1)} %all-gather.20.cloned.1.call-done, bf16[512,2048]{1,0:T(8,128)(2,1)S(1)} %bitcast.33, bf16[1,512,2048]{2,1,0:T(8,128)(2,1)} %all-gather.18.cloned.1.call-done, f32[512,512]{1,0:T(8,128)} %fusion.4), kind=kOutput, calls=%fused_computation.2 | convolution fusion | flops 2150105088 | bytes 9437184 | tf_op jit(solution)/shard_map/dot_general | solution.py:32
  127.6 4.7 %all-to-all-start.1 = ((bf16[8,64,2048]{2,1,0:T(8,128)(2,1)}), bf16[8,64,2048]{2,1,0:T(8,128)(2,1)S(1)}, u32[]{:S(2)}, u32[]{:S(2)}) async-start(bf16[8,64,2048]{2,1,0:T(8,128)(2,1)} %bitcast.31), calls=%async_computation.1 | async-start | bytes 4194304 | tf_op jit(solution)/shard_map/all_to_all | solution.py:87
  133.5 24.7 %all-gather.10.cloned.1.call-done = bf16[512,2048]{1,0:T(8,128)(2,1)} async-done(((bf16[128,2048]{1,0:T(8,128)(2,1)}), bf16[512,2048]{1,0:T(8,128)(2,1)}) %all-gather.10.cloned.1.call-update) | async-done | bytes 2097168 | tf_op jit(solution)/shard_map/all_gather | solution.py:101
  158.1 2.4 fusion.31
  160.6 20.8 %all-to-all-done.1 = bf16[8,64,2048]{2,1,0:T(8,128)(2,1)S(1)} async-done(((bf16[8,64,2048]{2,1,0:T(8,128)(2,1)}), bf16[8,64,2048]{2,1,0:T(8,128)(2,1)S(1)}, u32[]{:S(2)}, u32[]{:S(2)}) %all-to-all-start.1) | async-done | bytes 2097184 | tf_op jit(solution)/shard_map/all_to_all | solution.py:87
  181.4 2.3 gather_fusion
  183.7 1.7 gather.12
  185.5 4.1 %multiply_reduce_fusion = f32[128,2048]{1,0:T(8,128)S(1)} fusion(bf16[128,2,2048]{2,1,0:T(2,128)(2,1)S(1)} %gather.12, pred[128,2]{1,0:T(8,128)(4,1)S(1)} %copy.40, f32[128,2]{1,0:T(8,128)S(1)} %copy.35), kind=kLoop, calls=%fused_computation.11 | loop fusion | flops 1835008 | bytes 2098432 | tf_op jit(solution)/shard_map/reduce_sum | solution.py:91
  189.6 5.5 %all-gather.12.cloned.1.call-done = bf16[512,2048]{1,0:T(8,128)(2,1)} async-done(((bf16[128,2048]{1,0:T(8,128)(2,1)}), bf16[512,2048]{1,0:T(8,128)(2,1)}) %all-gather.12.cloned.1.call-update) | async-done | bytes 2097168 | tf_op jit(solution)/shard_map/all_gather | solution.py:101
  195.0 36.9 %all-gather.14.cloned.1.call-done = bf16[512,2048]{1,0:T(8,128)(2,1)} async-done(((bf16[128,2048]{1,0:T(8,128)(2,1)}), bf16[512,2048]{1,0:T(8,128)(2,1)}) %all-gather.14.cloned.1.call-update) | async-done | bytes 2097168 | tf_op jit(solution)/shard_map/all_gather | solution.py:104
  231.9 4.3 %fusion = bf16[128,2048]{1,0:T(8,128)(2,1)} fusion(f32[128,2048]{1,0:T(8,128)S(1)} %multiply_reduce_fusion, bf16[512,2048]{1,0:T(8,128)(2,1)} %all-gather.14.cloned.1.call-done, bf16[512,2048]{1,0:T(8,128)(2,1)} %all-gather.12.cloned.1.call-done, f32[128,512]{1,0:T(8,128)S(1)} %fusion.31, bf16[128,2048]{1,0:T(8,128)(2,1)S(1)} %copy-done, ...), kind=kOutput, calls=%fused_computation.5 | convolution fusion | flops 538836992 | bytes 6562304 | tf_op jit(solution)/shard_map/dot_general | solution.py:32
  (34 shorter events, 2.3 us)
Async XLA Ops:
  6.5 2.8 %copy-start.2 = (s32[128,2]{0,1:T(2,128)S(1)}, s32[128,2]{0,1:T(2,128)}, u32[]{:S(2)}) copy-start(s32[128,2]{0,1:T(2,128)} %param.12) | copy-start | bytes 3076
  6.5 40.6 %all-gather.16.cloned.1.call-start = ((), (), s32[]{:S(2)}) async-start(), calls=%async_computation.5 | async-start | bytes 2621440 | tf_op jit(solution)/shard_map/all_gather | solution.py:81
  7.3 76.9 %all-gather.18.cloned.1.call-start = ((), (), s32[]{:S(2)}) async-start(), calls=%async_computation.6 | async-start | bytes 2621440 | tf_op jit(solution)/shard_map/all_gather | solution.py:81
  8.0 113.2 %all-gather.20.cloned.1.call-start = ((), (), s32[]{:S(2)}) async-start(), calls=%async_computation.7 | async-start | bytes 2621440 | tf_op jit(solution)/shard_map/all_gather | solution.py:84
  8.7 149.4 %all-gather.10.cloned.1.call-start = ((), (), s32[]{:S(2)}) async-start(), calls=%async_computation.2 | async-start | bytes 2621440 | tf_op jit(solution)/shard_map/all_gather | solution.py:101
  9.9 2.2 copy-start
  9.9 2.5 %copy-start.1 = (f32[2048]{0:T(1024)S(1)}, f32[2048]{0:T(1024)}, u32[]{:S(2)}) copy-start(f32[2048]{0:T(1024)} %param.11) | copy-start | bytes 24580
  14.6 55.4 %all-to-all-start = ((bf16[8,64,2048]{2,1,0:T(8,128)(2,1)}), bf16[8,64,2048]{2,1,0:T(8,128)(2,1)S(1)}, u32[]{:S(2)}, u32[]{:S(2)}) async-start(bf16[8,64,2048]{2,1,0:T(8,128)(2,1)} %bitcast.1), calls=%async_computation | async-start | bytes 4194304 | tf_op jit(solution)/shard_map/all_to_all | solution.py:70
  20.9 174.1 %all-gather.12.cloned.1.call-start = ((), (), s32[]{:S(2)}) async-start(), calls=%async_computation.3 | async-start | bytes 2621440 | tf_op jit(solution)/shard_map/all_gather | solution.py:101
  127.6 5.7 %copy-start.3 = (f32[128,2]{0,1:T(2,128)S(1)}, f32[128,2]{0,1:T(2,128)}, u32[]{:S(2)}) copy-start(f32[128,2]{0,1:T(2,128)} %param.13) | copy-start | bytes 3076
  127.6 53.8 %all-to-all-start.1 = ((bf16[8,64,2048]{2,1,0:T(8,128)(2,1)}), bf16[8,64,2048]{2,1,0:T(8,128)(2,1)S(1)}, u32[]{:S(2)}, u32[]{:S(2)}) async-start(bf16[8,64,2048]{2,1,0:T(8,128)(2,1)} %bitcast.31), calls=%async_computation.1 | async-start | bytes 4194304 | tf_op jit(solution)/shard_map/all_to_all | solution.py:87
  132.4 99.6 %all-gather.14.cloned.1.call-start = ((), (), s32[]{:S(2)}) async-start(), calls=%async_computation.4 | async-start | bytes 2621440 | tf_op jit(solution)/shard_map/all_gather | solution.py:104
Sparse Core Ops, SparseCore 0:
  9.2 37.8 all-gather.15
  49.0 35.1 all-gather.17
  86.0 35.1 all-gather.19
  122.9 35.1 all-gather.9
  159.8 35.1 all-gather.11
  196.7 35.1 all-gather.13
where the time goes:
time: 243 us
  waiting for transfers between devices  187 us (77%)
  matrix products  19.4 us (8%)
  between operations  13.6 us (6%)
  starting transfers between devices  11.3 us (5%)
  local copies, waits for them, and re-layouts  7.09 us (3%)
  other arithmetic  4.61 us (2%)
    all_gather x2, waiting for transfers between devices, body(): lax.all_gather(x, 'tp', axis=0, tiled=True)  74 us
    all_gather x4, waiting for transfers between devices, body(): lax.all_gather(a, 'tp', axis=0, tiled=True)  65.8 us
    all_to_all x1, waiting for transfers between devices, body(): lax.all_to_all(outgoing, 'ep', split_axis=0, concat_axis=0, tiled=True)  22.9 us
    all_to_all x1, waiting for transfers between devices, body(): lax.all_to_all(results, 'ep', split_axis=0, concat_axis=0, tiled=True)  20.8 us
    dot_general x2, matrix products, add_down(): return jnp.dot(hidden, piece, preferred_element_type=jnp.float32)  10.7 us
    dot_general x2, matrix products, against(): lax.dot_general(rows, weight, (((1,), (1,)), ((), ())), preferred_element...  6.57 us
    all_to_all x1, starting transfers between devices, body(): lax.all_to_all(outgoing, 'ep', split_axis=0, concat_axis=0, tiled=True)  6.35 us
  transfers between devices with their start and end apart: 8, of which 8 were waited for; matrix products, arithmetic and copies ran while one was open for 11% of the time, Pallas kernels for 0%

commit v1 on v0

--- a/solution.py
+++ b/solution.py
@@ -1,6 +1,9 @@
 import jax
 import jax.numpy as jnp
 from jax import lax
+from jax.experimental import pallas as pl
+from jax.experimental.pallas import tpu as pltpu
+from jax.experimental.layout import Layout, with_layout_constraint
 from jax.sharding import PartitionSpec as P
 
 EPS = 1e-06
@@ -35,7 +38,7 @@
     return collect_rest(down, add_down, empty)
 
 
-def body(
+def exchange_body(
     tokens,
     norm_gain,
     expert_ids,
@@ -106,7 +109,178 @@
     return (routed + shared).astype(jnp.bfloat16)
 
 
+CORES = 2
+CHUNKS = 4
+
+
+def copy_blocks(jobs, arrays, shapes, at=None):
+    def kernel(at_ref, *refs):
+        ins, outs, sem = refs[: len(arrays)], refs[len(arrays) : -1], refs[-1]
+        copies = []
+        for n, (source, row, rows, cols, target, to) in enumerate(jobs):
+            if row is None:
+                row = pl.multiple_of(at_ref[0], rows)
+            copies.append(
+                pltpu.make_async_copy(
+                    ins[source].at[pl.ds(row, rows), cols],
+                    outs[target].at[pl.ds(to, rows)],
+                    sem.at[n],
+                )
+            )
+        for copy in copies:
+            copy.start()
+        for copy in copies:
+            copy.wait()
+
+    at = jnp.zeros((1,), jnp.int32) if at is None else at
+    moved = sum(s[0] * s[1] for s in shapes) * 2
+    return pl.pallas_call(
+        kernel,
+        out_shape=[jax.ShapeDtypeStruct(s, jnp.bfloat16) for s in shapes],
+        in_specs=[pl.BlockSpec(memory_space=pltpu.SMEM)]
+        + [pl.BlockSpec(memory_space=pltpu.HBM)] * len(arrays),
+        out_specs=[pl.BlockSpec(memory_space=pltpu.VMEM)] * len(shapes),
+        scratch_shapes=[pltpu.SemaphoreType.DMA((len(jobs),))],
+        compiler_params=pltpu.CompilerParams(vmem_limit_bytes=8 * 1024 * 1024),
+        cost_estimate=pl.CostEstimate(flops=moved, bytes_accessed=2 * moved, transcendentals=0),
+    )(at, *arrays)
+
+
+def column_body(
+    tokens,
+    norm_gain,
+    expert_ids,
+    gate_weights,
+    expert_gate,
+    expert_up,
+    expert_down,
+    shared_gate,
+    shared_up,
+    shared_down,
+):
+    ep, tp = lax.axis_size("ep"), lax.axis_size("tp")
+    levels = ep // CORES
+    me = lax.axis_index("ep")
+    tok_rows, features = tokens.shape
+
+    z_up = [(i, (i + CORES) % ep) for i in range(ep)]
+    swap = [(i, i ^ 1) for i in range(ep)]
+    x_swap = [(i, i ^ 1) for i in range(tp)]
+    y_swap = [(i, i ^ 2) for i in range(tp)]
+    both_swap = [(i, i ^ 3) for i in range(tp)]
+
+    def over_x(a):
+        return lax.ppermute(a, "tp", x_swap)
+
+    def over_y(a):
+        return lax.ppermute(a, "tp", y_swap)
+
+    def across(a):
+        return lax.ppermute(a, "tp", both_swap)
+
+    def up(a):
+        return lax.ppermute(a, "ep", z_up)
+
+    def other_core(a):
+        return lax.ppermute(a, "ep", swap)
+
+    s = shared_gate.shape[0] // ep
+    features = tokens.shape[1]
+    every = slice(0, features)
+    shared = copy_blocks(
+        [(i, None, s, every, 0, i * s) for i in range(3)],
+        (shared_gate, shared_up, shared_down),
+        [(3 * s, features)],
+        at=(me * s).astype(jnp.int32)[None],
+    )[0]
+    gate, upw, down = expert_gate[0], expert_up[0], expert_down[0]
+
+    labels = jnp.arange(ep, dtype=jnp.int32)[:, None]
+    dense = sum(
+        jnp.where(expert_ids[None, :, k] == labels, gate_weights[None, :, k], 0.0)
+        for k in range(expert_ids.shape[1])
+    )
+
+    gx, gy = over_x(gate), over_y(gate)
+    ux, uy = over_x(upw), over_y(upw)
+    sx, sy, sd = over_x(shared), over_y(shared), across(shared)
+    gd, ud = over_y(gx), over_x(uy)
+
+    own_blocks, other_blocks = [tokens], [other_core(tokens)]
+    weights = [jnp.concatenate([dense, other_core(dense)], axis=0)]
+    for _ in range(1, levels):
+        own_blocks.append(up(own_blocks[-1]))
+        other_blocks.append(other_core(own_blocks[-1]))
+        weights.append(up(weights[-1]))
+
+    quarter = features // CHUNKS
+    down_rows = []
+    for n, (lo, hi) in enumerate(((0, 1), (1, 2), (2, 4))):
+        piece = down[:, lo * quarter : hi * quarter]
+        dx, dy = over_x(piece), over_y(piece)
+        dd = across(piece)
+        down_rows.append((piece, dx, dy, dd))
+
+    def normed_of(part):
+        tok = part.astype(jnp.float32)
+        factor = lax.rsqrt(jnp.mean(tok * tok, axis=-1, keepdims=True) + EPS)
+        return (tok * factor * norm_gain).astype(jnp.bfloat16)
+
+    def joined(pieces):
+        return jnp.concatenate(pieces, axis=0)
+
+    order = list(range(1, levels)) + [0]
+    shares = (shared, sx, sy, sd)
+    n = gate.shape[0]
+    units = 4 * n + 4 * s
+    places = (0, n, 2 * n, 3 * n)
+    arrays = (gate, gx, gy, gd, upw, ux, uy, ud, *shares)
+    jobs = [(i, 0, n, every, i // 4, places[i % 4]) for i in range(8)]
+    jobs += [(8 + i, t * s, s, every, t, 4 * n + i * s) for i in range(4) for t in range(2)]
+    g_all, u_all = copy_blocks(jobs, arrays, [(units, features)] * 2)
+    weights = lax.optimization_barrier((*weights, g_all))[:-1]
+
+    rows = joined(
+        [normed_of(own_blocks[r]) for r in order] + [normed_of(other_blocks[r]) for r in order]
+    )
+    picked = [lax.dynamic_slice_in_dim(weights[r].reshape(2, ep, -1), me, 1, 1) for r in order]
+    scale = joined([p[c, 0] for c in range(2) for p in picked])[:, None]
+    routed = (jnp.arange(units) < 4 * n)[None, :]
+    value = jax.nn.silu(against(rows, g_all)) * against(rows, u_all)
+    hidden = (value * jnp.where(routed, scale, 1.0)).astype(jnp.bfloat16)
+
+    own_rows = levels * tok_rows
+
+    def product(c, lo, hi):
+        arrays = (*down_rows[c], *shares)
+        jobs = [(i, 0, n, slice(0, hi - lo), 0, i * n) for i in range(4)]
+        jobs += [(4 + i, 2 * s, s, slice(lo, hi), 0, 4 * n + i * s) for i in range(4)]
+        down_all = copy_blocks(jobs, arrays, [(units, hi - lo)])[0]
+        part = jnp.dot(hidden, down_all, preferred_element_type=jnp.float32)
+        return with_layout_constraint(part, Layout(major_to_minor=(0, 1)))
+
+    parts = [product(0, 0, quarter), product(1, quarter, 2 * quarter)]
+    wide = product(2, 2 * quarter, features)
+    parts += [wide[:, :quarter], wide[:, quarter:]]
+    outs = []
+    for part in parts:
+        swapped = other_core(part[own_rows:].astype(jnp.bfloat16))
+        total = part[:own_rows] + swapped.astype(jnp.float32)
+        moving = total[:tok_rows]
+        for r in range(1, levels):
+            arrived = up(moving.astype(jnp.bfloat16))
+            moving = total[r * tok_rows : (r + 1) * tok_rows] + arrived.astype(jnp.float32)
+        outs.append(moving.astype(jnp.bfloat16))
+    return jnp.concatenate(outs, axis=1)
+
+
 def solution(mesh):
+    ep, tp = mesh.shape["ep"], mesh.shape["tp"]
+    columns = tp == 4 and ep == 4 * CORES
+
+    def body(*args):
+        return (column_body if columns else exchange_body)(*args)
+
     in_specs = (
         P(("ep", "tp"), None),
         P(),
@@ -120,4 +294,6 @@
         P("tp", None),
     )
     out_specs = P(("ep", "tp"), None)
-    return jax.shard_map(body, mesh=mesh, in_specs=in_specs, out_specs=out_specs, check_vma=False)
+    return jax.shard_map(
+        body, mesh=mesh, in_specs=in_specs, out_specs=out_specs, check_vma=False
+    )

time: 243 us -> 165 us (0.68)
  waiting for transfers between devices: 187 us -> 94.1 us
  starting transfers between devices: 11.3 us -> 37.2 us
  between operations: 13.6 us -> 0.58 us
  matrix products: 19.4 us -> 9.63 us
  other arithmetic: 4.61 us -> 9.84 us
  Pallas kernels: 0 us -> 3.87 us
    all_gather x6 -> x0, waiting for transfers between devices: 140 us -> none  [the longest x2 74 us: body(): lax.all_gather(x, 'tp', axis=0, tiled=True)]
    ppermute x0 -> x45, waiting for transfers between devices: none -> 94.1 us  [the longest x18 61 us: up(): return lax.ppermute(a, 'ep', z_up)]
    all_to_all x2 -> x0, waiting for transfers between devices: 43.7 us -> none  [the longest x1 22.9 us: body(): lax.all_to_all(outgoing, 'ep', split_axis=0, concat_axis=0, tiled=True)]
    ppermute x0 -> x45, starting transfers between devices: none -> 37.2 us  [the longest x18 10.9 us: up(): return lax.ppermute(a, 'ep', z_up)]
    all_to_all x2 -> x0, starting transfers between devices: 11.1 us -> none  [the longest x1 6.35 us: body(): lax.all_to_all(outgoing, 'ep', split_axis=0, concat_axis=0, tiled=True)]
    dot_general x3, matrix products: 12.8 us -> 3.86 us  [product(): part = jnp.dot(hidden, down_all, preferred_element_type=jnp.float32)]
    gather x7 -> x0, local copies, waits for them, and re-layouts: 6.47 us -> none  [the longest x2 4.08 us: body(): jnp.take(returned, flat_pos.reshape(-1), axis=0)]
    unnamed x9 -> x31, local copies, waits for them, and re-layouts: 0.13 us -> 6.36 us
  transfers between devices with their start and end apart: 8 -> 45, of which waited for: 8 -> 23; matrix products, arithmetic and copies ran while one was open for 11% -> 7% of each run, Pallas kernels for 0% -> 2%
where the time goes in v1:
time: 165 us; the launch traced here: 164 us
  waiting for transfers between devices  94.1 us (57%)
  starting transfers between devices  37.2 us (23%)
  other arithmetic  9.84 us (6%)
  matrix products  9.63 us (6%)
  local copies, waits for them, and re-layouts  9.23 us (6%)
  Pallas kernels  3.87 us (2%)
    ppermute x18, waiting for transfers between devices, up(): return lax.ppermute(a, 'ep', z_up)  61 us
    ppermute x7, waiting for transfers between devices, over_x(): return lax.ppermute(a, 'tp', x_swap)  13.3 us
    ppermute x18, starting transfers between devices, up(): return lax.ppermute(a, 'ep', z_up)  10.9 us
    ppermute x4, waiting for transfers between devices, across(): return lax.ppermute(a, 'tp', both_swap)  10.8 us
    ppermute x7, starting transfers between devices, over_x(): return lax.ppermute(a, 'tp', x_swap)  9.7 us
    ppermute x7, waiting for transfers between devices, over_y(): return lax.ppermute(a, 'tp', y_swap)  8.64 us
    ppermute x4, starting transfers between devices, across(): return lax.ppermute(a, 'tp', both_swap)  8.13 us
    ppermute x7, starting transfers between devices, over_y(): return lax.ppermute(a, 'tp', y_swap)  6.99 us
  transfers between devices with their start and end apart: 45, of which 23 were waited for; matrix products, arithmetic and copies ran while one was open for 7% of the time, Pallas kernels for 2%

profile of v1, /device:TPU:0, one launch (start us, length us, event | category | flops | bytes accessed | tf_op | source)
XLA Modules:
  0.0 164.4 jit_solution(7862434896220575651)
XLA Ops:
  1.1 3.0 %collective-permute-start.27 = (bf16[128,512]{1,0:T(8,128)(2,1)S(1)}, bf16[128,512]{1,0:T(8,128)(2,1)S(1)}, u32[]{:S(2)}, u32[]{:S(2)}) collective-permute-start(bf16[128,512]{1,0:T(8,128)(2,1)S(1)} %get-tuple-element.22.refs_0_), channel_id=1, source_target_pairs={{0,1},{1,0},{2,3},{3,2},{4,5},{5,4},{6,7},{7,6},{8,9},{9,8},{10,11... | collective-permute-start | bytes 393224 | tf_op jit(solution)/shard_map/ppermute | solution.py:173
  18.2 2.9 %collective-permute-done.20.refs_1_ = bf16[128,512]{1,0:T(8,128)(2,1)S(1)} collective-permute-done((bf16[128,512]{1,0:T(8,128)(2,1)S(1)}, bf16[128,512]{1,0:T(8,128)(2,1)S(1)}, u32[]{:S(2)}, u32[]{:S(2)}) %collective-permute-start.20) | collective-permute-done | bytes 131104 | tf_op jit(solution)/shard_map/ppermute | solution.py:173
  30.3 2.7 %collective-permute-start.22 = (bf16[128,512]{1,0:T(8,128)(2,1)S(1)}, bf16[128,512]{1,0:T(8,128)(2,1)}, u32[]{:S(2)}, u32[]{:S(2)}) collective-permute-start(bf16[128,512]{1,0:T(8,128)(2,1)S(1)} %get-tuple-element.21.refs_0_), channel_id=1, source_target_pairs={{0,3},{1,2},{2,1},{3,0},{4,7},{5,6},{6,5},{7,4},{8,11},{9,10},{10,... | collective-permute-start | bytes 393224 | tf_op jit(solution)/shard_map/ppermute | solution.py:179
  34.4 9.0 %collective-permute-done.22.refs_3_ = bf16[128,512]{1,0:T(8,128)(2,1)} collective-permute-done((bf16[128,512]{1,0:T(8,128)(2,1)S(1)}, bf16[128,512]{1,0:T(8,128)(2,1)}, u32[]{:S(2)}, u32[]{:S(2)}) %collective-permute-start.22) | collective-permute-done | bytes 131104 | tf_op jit(solution)/shard_map/ppermute | solution.py:179
  56.2 11.3 %collective-permute-done.17 = f32[16,128]{1,0:T(8,128)S(1)} collective-permute-done((f32[16,128]{1,0:T(8,128)S(1)}, f32[16,128]{1,0:T(8,128)S(1)}, u32[]{:S(2)}, u32[]{:S(2)}) %collective-permute-start.17) | collective-permute-done | bytes 8224 | tf_op jit(solution)/shard_map/ppermute | solution.py:182
  68.2 5.3 %collective-permute-done.18 = f32[16,128]{1,0:T(8,128)S(1)} collective-permute-done((f32[16,128]{1,0:T(8,128)S(1)}, f32[16,128]{1,0:T(8,128)S(1)}, u32[]{:S(2)}, u32[]{:S(2)}) %collective-permute-start.18) | collective-permute-done | bytes 8224 | tf_op jit(solution)/shard_map/ppermute | solution.py:182
  77.3 5.0 %collective-permute-done.8.refs_2_ = bf16[128,2048]{1,0:T(8,128)(2,1)S(1)} collective-permute-done((bf16[128,2048]{1,0:T(8,128)(2,1)S(1)}, bf16[128,2048]{1,0:T(8,128)(2,1)S(1)}, u32[]{:S(2)}, u32[]{:S(2)}) %collective-permute-start.8) | collective-permute-done | bytes 524320 | tf_op jit(solution)/shard_map/ppermute | solution.py:176
  82.3 5.9 %collective-permute-done.10.refs_5_ = bf16[128,2048]{1,0:T(8,128)(2,1)S(1)} collective-permute-done((bf16[128,2048]{1,0:T(8,128)(2,1)S(1)}, bf16[128,2048]{1,0:T(8,128)(2,1)S(1)}, u32[]{:S(2)}, u32[]{:S(2)}) %collective-permute-start.10) | collective-permute-done | bytes 524320 | tf_op jit(solution)/shard_map/ppermute | solution.py:173
  88.2 3.6 %collective-permute-done.9.refs_3_ = bf16[128,2048]{1,0:T(8,128)(2,1)S(1)} collective-permute-done((bf16[128,2048]{1,0:T(8,128)(2,1)S(1)}, bf16[128,2048]{1,0:T(8,128)(2,1)S(1)}, u32[]{:S(2)}, u32[]{:S(2)}) %collective-permute-start.9) | collective-permute-done | bytes 524320 | tf_op jit(solution)/shard_map/ppermute | solution.py:176
  91.8 4.5 %collective-permute-done.12.refs_7_ = bf16[128,2048]{1,0:T(8,128)(2,1)S(1)} collective-permute-done((bf16[128,2048]{1,0:T(8,128)(2,1)S(1)}, bf16[128,2048]{1,0:T(8,128)(2,1)S(1)}, u32[]{:S(2)}, u32[]{:S(2)}) %collective-permute-start.12) | collective-permute-done | bytes 524320 | tf_op jit(solution)/shard_map/ppermute | solution.py:173
  98.1 12.3 %collective-permute-done.2 = bf16[128,2048]{1,0:T(8,128)(2,1)S(1)} collective-permute-done((bf16[128,2048]{1,0:T(8,128)(2,1)S(1)}, bf16[128,2048]{1,0:T(8,128)(2,1)S(1)}, u32[]{:S(2)}, u32[]{:S(2)}) %collective-permute-start.2) | collective-permute-done | bytes 524320 | tf_op jit(solution)/shard_map/ppermute | solution.py:182
  113.4 2.7 %fusion.55 = f32[1024,576]{0,1:T(8,128)S(1)} fusion(bf16[1024,2048]{1,0:T(8,128)(2,1)S(1)} %fusion.24, bf16[576,2048]{1,0:T(8,128)(2,1)S(1)} %get-tuple-element.11), kind=kOutput, calls=%fused_computation.128 | convolution fusion | flops 2415919104 | bytes 8912896 | tf_op jit(solution)/shard_map/dot_general | solution.py:17
  116.1 3.0 %multiply_convert_fusion = bf16[1024,576]{0,1:T(8,128)(2,1)S(1)} fusion(f32[1024,576]{0,1:T(8,128)S(1)} %fusion.55, f32[1024]{0:T(1024)S(1)} %constant_dynamic-update-slice_fusion.1, pred[576]{0:T(1024)(128)(4,1)S(1)} %copy-done.11, bf16[1024,2048]{1,0:T(8,128)(2,1)S(1)} %fusion.24, bf16[576,2048]{1,0:T(8,128)(2,1)S(1)} %get-tuple-element.12), kind=kOutput, calls=%fused_computation | convolution fusion | flops 2420637696 | bytes 10097216 | tf_op jit(solution)/shard_map/dot_general | solution.py:17
  126.6 4.0 %collective-permute-start.24 = (bf16[128,512]{1,0:T(8,128)(2,1)S(1)}, bf16[128,512]{1,0:T(8,128)(2,1)S(1)}, u32[]{:S(2)}, u32[]{:S(2)}) collective-permute-start(bf16[128,512]{1,0:T(8,128)(2,1)S(1)} %slice.252), channel_id=1, source_target_pairs={{0,8},{4,12},{8,16},{12,20},{16,24},{20,28},{24,0},{28,4},{1,9},{5... | collective-permute-start | bytes 393224 | tf_op jit(solution)/shard_map/ppermute | solution.py:182
  133.3 2.7 %collective-permute-done.38 = bf16[128,512]{1,0:T(8,128)(2,1)S(1)} collective-permute-done((bf16[128,512]{1,0:T(8,128)(2,1)S(1)}, bf16[128,512]{1,0:T(8,128)(2,1)S(1)}, u32[]{:S(2)}, u32[]{:S(2)}) %collective-permute-start.38) | collective-permute-done | bytes 131104 | tf_op jit(solution)/shard_map/ppermute | solution.py:182
  136.1 2.7 %collective-permute-done.31 = bf16[128,512]{1,0:T(8,128)(2,1)S(1)} collective-permute-done((bf16[128,512]{1,0:T(8,128)(2,1)S(1)}, bf16[128,512]{1,0:T(8,128)(2,1)S(1)}, u32[]{:S(2)}, u32[]{:S(2)}) %collective-permute-start.31) | collective-permute-done | bytes 131104 | tf_op jit(solution)/shard_map/ppermute | solution.py:182
  138.9 2.7 %collective-permute-done.24 = bf16[128,512]{1,0:T(8,128)(2,1)S(1)} collective-permute-done((bf16[128,512]{1,0:T(8,128)(2,1)S(1)}, bf16[128,512]{1,0:T(8,128)(2,1)S(1)}, u32[]{:S(2)}, u32[]{:S(2)}) %collective-permute-start.24) | collective-permute-done | bytes 131104 | tf_op jit(solution)/shard_map/ppermute | solution.py:182
  141.7 2.7 %collective-permute-done.43 = bf16[128,512]{1,0:T(8,128)(2,1)S(1)} collective-permute-done((bf16[128,512]{1,0:T(8,128)(2,1)S(1)}, bf16[128,512]{1,0:T(8,128)(2,1)S(1)}, u32[]{:S(2)}, u32[]{:S(2)}) %collective-permute-start.43) | collective-permute-done | bytes 131104 | tf_op jit(solution)/shard_map/ppermute | solution.py:182
  144.5 2.7 %collective-permute-done.39 = bf16[128,512]{1,0:T(8,128)(2,1)S(1)} collective-permute-done((bf16[128,512]{1,0:T(8,128)(2,1)S(1)}, bf16[128,512]{1,0:T(8,128)(2,1)S(1)}, u32[]{:S(2)}, u32[]{:S(2)}) %collective-permute-start.39) | collective-permute-done | bytes 131104 | tf_op jit(solution)/shard_map/ppermute | solution.py:182
  147.3 2.7 %collective-permute-done.32 = bf16[128,512]{1,0:T(8,128)(2,1)S(1)} collective-permute-done((bf16[128,512]{1,0:T(8,128)(2,1)S(1)}, bf16[128,512]{1,0:T(8,128)(2,1)S(1)}, u32[]{:S(2)}, u32[]{:S(2)}) %collective-permute-start.32) | collective-permute-done | bytes 131104 | tf_op jit(solution)/shard_map/ppermute | solution.py:182
  150.1 2.7 %collective-permute-done.25 = bf16[128,512]{1,0:T(8,128)(2,1)S(1)} collective-permute-done((bf16[128,512]{1,0:T(8,128)(2,1)S(1)}, bf16[128,512]{1,0:T(8,128)(2,1)S(1)}, u32[]{:S(2)}, u32[]{:S(2)}) %collective-permute-start.25) | collective-permute-done | bytes 131104 | tf_op jit(solution)/shard_map/ppermute | solution.py:182
  153.0 2.7 %collective-permute-done.44 = bf16[128,512]{1,0:T(8,128)(2,1)S(1)} collective-permute-done((bf16[128,512]{1,0:T(8,128)(2,1)S(1)}, bf16[128,512]{1,0:T(8,128)(2,1)S(1)}, u32[]{:S(2)}, u32[]{:S(2)}) %collective-permute-start.44) | collective-permute-done | bytes 131104 | tf_op jit(solution)/shard_map/ppermute | solution.py:182
  155.7 2.8 %collective-permute-done.40 = bf16[128,512]{1,0:T(8,128)(2,1)S(1)} collective-permute-done((bf16[128,512]{1,0:T(8,128)(2,1)S(1)}, bf16[128,512]{1,0:T(8,128)(2,1)S(1)}, u32[]{:S(2)}, u32[]{:S(2)}) %collective-permute-start.40) | collective-permute-done | bytes 131104 | tf_op jit(solution)/shard_map/ppermute | solution.py:182
  158.5 2.8 %collective-permute-done.33 = bf16[128,512]{1,0:T(8,128)(2,1)S(1)} collective-permute-done((bf16[128,512]{1,0:T(8,128)(2,1)S(1)}, bf16[128,512]{1,0:T(8,128)(2,1)S(1)}, u32[]{:S(2)}, u32[]{:S(2)}) %collective-permute-start.33) | collective-permute-done | bytes 131104 | tf_op jit(solution)/shard_map/ppermute | solution.py:182
  (163 shorter events, 61.4 us)
Async XLA Ops:
  1.1 13.2 %collective-permute-start.27 = (bf16[128,512]{1,0:T(8,128)(2,1)S(1)}, bf16[128,512]{1,0:T(8,128)(2,1)S(1)}, u32[]{:S(2)}, u32[]{:S(2)}) collective-permute-start(bf16[128,512]{1,0:T(8,128)(2,1)S(1)} %get-tuple-element.22.refs_0_), channel_id=1, source_target_pairs={{0,1},{1,0},{2,3},{3,2},{4,5},{5,4},{6,7},{7,6},{8,9},{9,8},{10,11... | collective-permute-start | bytes 393224 | tf_op jit(solution)/shard_map/ppermute | solution.py:173
  10.6 14.9 %collective-permute-start.13 = (bf16[48,2048]{1,0:T(8,128)(2,1)S(1)}, bf16[48,2048]{1,0:T(8,128)(2,1)S(1)}, u32[]{:S(2)}, u32[]{:S(2)}) collective-permute-start(bf16[48,2048]{1,0:T(8,128)(2,1)S(1)} %shard_map.100.refs_8_.refs_4_), channel_id=1, source_target_pairs={{0,1},{1,0},{2,3},{3,2},{4,5},{5,4},{6,7},{7,6},{8,9},{9,8},{10,11... | collective-permute-start | bytes 589832 | tf_op jit(solution)/shard_map/ppermute | solution.py:173
  12.7 13.2 %collective-permute-start.14 = (bf16[48,2048]{1,0:T(8,128)(2,1)S(1)}, bf16[48,2048]{1,0:T(8,128)(2,1)S(1)}, u32[]{:S(2)}, u32[]{:S(2)}) collective-permute-start(bf16[48,2048]{1,0:T(8,128)(2,1)S(1)} %shard_map.100.refs_8_.refs_4_), channel_id=1, source_target_pairs={{0,2},{1,3},{2,0},{3,1},{4,6},{5,7},{6,4},{7,5},{8,10},{9,11},{10,... | collective-permute-start | bytes 589832 | tf_op jit(solution)/shard_map/ppermute | solution.py:176
  14.9 35.2 %collective-permute-start = (bf16[128,2048]{1,0:T(8,128)(2,1)}, bf16[128,2048]{1,0:T(8,128)(2,1)}, u32[]{:S(2)}, u32[]{:S(2)}) collective-permute-start(bf16[128,2048]{1,0:T(8,128)(2,1)} %param.10), channel_id=1, source_target_pairs={{0,8},{4,12},{8,16},{12,20},{16,24},{20,28},{24,0},{28,4},{1,9},{5... | collective-permute-start | bytes 1572872 | tf_op jit(solution)/shard_map/ppermute | solution.py:182
  25.0 21.7 %collective-permute-start.34 = (bf16[128,1024]{1,0:T(8,128)(2,1)S(1)}, bf16[128,1024]{1,0:T(8,128)(2,1)S(1)}, u32[]{:S(2)}, u32[]{:S(2)}) collective-permute-start(bf16[128,1024]{1,0:T(8,128)(2,1)S(1)} %slice.184.refs_0_), channel_id=1, source_target_pairs={{0,1},{1,0},{2,3},{3,2},{4,5},{5,4},{6,7},{7,6},{8,9},{9,8},{10,11... | collective-permute-start | bytes 786440 | tf_op jit(solution)/shard_map/ppermute | solution.py:173
  25.6 22.7 %collective-permute-start.35 = (bf16[128,1024]{1,0:T(8,128)(2,1)S(1)}, bf16[128,1024]{1,0:T(8,128)(2,1)S(1)}, u32[]{:S(2)}, u32[]{:S(2)}) collective-permute-start(bf16[128,1024]{1,0:T(8,128)(2,1)S(1)} %slice.184.refs_0_), channel_id=1, source_target_pairs={{0,2},{1,3},{2,0},{3,1},{4,6},{5,7},{6,4},{7,5},{8,10},{9,11},{10,... | collective-permute-start | bytes 786440 | tf_op jit(solution)/shard_map/ppermute | solution.py:176
  25.8 24.0 %collective-permute-start.36 = (bf16[128,1024]{1,0:T(8,128)(2,1)S(1)}, bf16[128,1024]{1,0:T(8,128)(2,1)S(1)}, u32[]{:S(2)}, u32[]{:S(2)}) collective-permute-start(bf16[128,1024]{1,0:T(8,128)(2,1)S(1)} %slice.184.refs_0_), channel_id=1, source_target_pairs={{0,3},{1,2},{2,1},{3,0},{4,7},{5,6},{6,5},{7,4},{8,11},{9,10},{10,... | collective-permute-start | bytes 786440 | tf_op jit(solution)/shard_map/ppermute | solution.py:179
  30.3 13.1 %collective-permute-start.22 = (bf16[128,512]{1,0:T(8,128)(2,1)S(1)}, bf16[128,512]{1,0:T(8,128)(2,1)}, u32[]{:S(2)}, u32[]{:S(2)}) collective-permute-start(bf16[128,512]{1,0:T(8,128)(2,1)S(1)} %get-tuple-element.21.refs_0_), channel_id=1, source_target_pairs={{0,3},{1,2},{2,1},{3,0},{4,7},{5,6},{6,5},{7,4},{8,11},{9,10},{10,... | collective-permute-start | bytes 393224 | tf_op jit(solution)/shard_map/ppermute | solution.py:179
  46.8 27.2 %collective-permute-start.7 = (bf16[128,2048]{1,0:T(8,128)(2,1)S(1)}, bf16[128,2048]{1,0:T(8,128)(2,1)S(1)}, u32[]{:S(2)}, u32[]{:S(2)}) collective-permute-start(bf16[128,2048]{1,0:T(8,128)(2,1)S(1)} %bitcast.58), channel_id=1, source_target_pairs={{0,1},{1,0},{2,3},{3,2},{4,5},{5,4},{6,7},{7,6},{8,9},{9,8},{10,11... | collective-permute-start | bytes 1572872 | tf_op jit(solution)/shard_map/ppermute | solution.py:173
  48.3 25.7 %collective-permute-start.11 = (bf16[128,2048]{1,0:T(8,128)(2,1)S(1)}, bf16[128,2048]{1,0:T(8,128)(2,1)S(1)}, u32[]{:S(2)}, u32[]{:S(2)}) collective-permute-start(bf16[128,2048]{1,0:T(8,128)(2,1)S(1)} %bitcast.61), channel_id=1, source_target_pairs={{0,2},{1,3},{2,0},{3,1},{4,6},{5,7},{6,4},{7,5},{8,10},{9,11},{10,... | collective-permute-start | bytes 1572872 | tf_op jit(solution)/shard_map/ppermute | solution.py:176
  51.3 16.7 %collective-permute-start.1 = (bf16[128,2048]{1,0:T(8,128)(2,1)}, bf16[128,2048]{1,0:T(8,128)(2,1)S(1)}, u32[]{:S(2)}, u32[]{:S(2)}) collective-permute-start(bf16[128,2048]{1,0:T(8,128)(2,1)} %collective-permute-done), channel_id=1, source_target_pairs={{0,8},{4,12},{8,16},{12,20},{16,24},{20,28},{24,0},{28,4},{1,9},{5... | collective-permute-start | bytes 1572872 | tf_op jit(solution)/shard_map/ppermute | solution.py:182
  53.1 22.5 %collective-permute-start.3 = (bf16[128,2048]{1,0:T(8,128)(2,1)}, bf16[128,2048]{1,0:T(8,128)(2,1)S(1)}, u32[]{:S(2)}, u32[]{:S(2)}) collective-permute-start(bf16[128,2048]{1,0:T(8,128)(2,1)} %collective-permute-done), channel_id=1, source_target_pairs={{0,4},{4,0},{8,12},{12,8},{16,20},{20,16},{24,28},{28,24},{1,5},{5... | collective-permute-start | bytes 1572872 | tf_op jit(solution)/shard_map/ppermute | solution.py:185
  54.3 13.2 %collective-permute-start.17 = (f32[16,128]{1,0:T(8,128)S(1)}, f32[16,128]{1,0:T(8,128)S(1)}, u32[]{:S(2)}, u32[]{:S(2)}) collective-permute-start(f32[16,128]{1,0:T(8,128)S(1)} %pad_maximum_fusion.1), channel_id=1, source_target_pairs={{0,8},{4,12},{8,16},{12,20},{16,24},{20,28},{24,0},{28,4},{1,9},{5... | collective-permute-start | bytes 24584 | tf_op jit(solution)/shard_map/ppermute | solution.py:182
  67.5 14.8 %collective-permute-start.8 = (bf16[128,2048]{1,0:T(8,128)(2,1)S(1)}, bf16[128,2048]{1,0:T(8,128)(2,1)S(1)}, u32[]{:S(2)}, u32[]{:S(2)}) collective-permute-start(bf16[128,2048]{1,0:T(8,128)(2,1)S(1)} %bitcast.59), channel_id=1, source_target_pairs={{0,2},{1,3},{2,0},{3,1},{4,6},{5,7},{6,4},{7,5},{8,10},{9,11},{10,... | collective-permute-start | bytes 1572872 | tf_op jit(solution)/shard_map/ppermute | solution.py:176
  73.4 14.8 %collective-permute-start.10 = (bf16[128,2048]{1,0:T(8,128)(2,1)S(1)}, bf16[128,2048]{1,0:T(8,128)(2,1)S(1)}, u32[]{:S(2)}, u32[]{:S(2)}) collective-permute-start(bf16[128,2048]{1,0:T(8,128)(2,1)S(1)} %bitcast.62), channel_id=1, source_target_pairs={{0,1},{1,0},{2,3},{3,2},{4,5},{5,4},{6,7},{7,6},{8,9},{9,8},{10,11... | collective-permute-start | bytes 1572872 | tf_op jit(solution)/shard_map/ppermute | solution.py:173
  74.0 23.5 %collective-permute-start.19 = (f32[16,128]{1,0:T(8,128)S(1)}, f32[16,128]{1,0:T(8,128)S(1)}, u32[]{:S(2)}, u32[]{:S(2)}) collective-permute-start(f32[16,128]{1,0:T(8,128)S(1)} %collective-permute-done.18), channel_id=1, source_target_pairs={{0,8},{4,12},{8,16},{12,20},{16,24},{20,28},{24,0},{28,4},{1,9},{5... | collective-permute-start | bytes 24584 | tf_op jit(solution)/shard_map/ppermute | solution.py:182
  74.0 17.9 %collective-permute-start.9 = (bf16[128,2048]{1,0:T(8,128)(2,1)S(1)}, bf16[128,2048]{1,0:T(8,128)(2,1)S(1)}, u32[]{:S(2)}, u32[]{:S(2)}) collective-permute-start(bf16[128,2048]{1,0:T(8,128)(2,1)S(1)} %collective-permute-done.7.refs_1_), channel_id=1, source_target_pairs={{0,2},{1,3},{2,0},{3,1},{4,6},{5,7},{6,4},{7,5},{8,10},{9,11},{10,... | collective-permute-start | bytes 1572872 | tf_op jit(solution)/shard_map/ppermute | solution.py:176
  75.6 20.7 %collective-permute-start.12 = (bf16[128,2048]{1,0:T(8,128)(2,1)S(1)}, bf16[128,2048]{1,0:T(8,128)(2,1)S(1)}, u32[]{:S(2)}, u32[]{:S(2)}) collective-permute-start(bf16[128,2048]{1,0:T(8,128)(2,1)S(1)} %collective-permute-done.11.refs_6_), channel_id=1, source_target_pairs={{0,1},{1,0},{2,3},{3,2},{4,5},{5,4},{6,7},{7,6},{8,9},{9,8},{10,11... | collective-permute-start | bytes 1572872 | tf_op jit(solution)/shard_map/ppermute | solution.py:173
  97.6 12.8 %collective-permute-start.2 = (bf16[128,2048]{1,0:T(8,128)(2,1)S(1)}, bf16[128,2048]{1,0:T(8,128)(2,1)S(1)}, u32[]{:S(2)}, u32[]{:S(2)}) collective-permute-start(bf16[128,2048]{1,0:T(8,128)(2,1)S(1)} %collective-permute-done.1), channel_id=1, source_target_pairs={{0,8},{4,12},{8,16},{12,20},{16,24},{20,28},{24,0},{28,4},{1,9},{5... | collective-permute-start | bytes 1572872 | tf_op jit(solution)/shard_map/ppermute | solution.py:182
  97.9 14.3 %collective-permute-start.4 = (bf16[128,2048]{1,0:T(8,128)(2,1)S(1)}, bf16[128,2048]{1,0:T(8,128)(2,1)S(1)}, u32[]{:S(2)}, u32[]{:S(2)}) collective-permute-start(bf16[128,2048]{1,0:T(8,128)(2,1)S(1)} %collective-permute-done.1), channel_id=1, source_target_pairs={{0,4},{4,0},{8,12},{12,8},{16,20},{20,16},{24,28},{28,24},{1,5},{5... | collective-permute-start | bytes 1572872 | tf_op jit(solution)/shard_map/ppermute | solution.py:185
  125.3 13.5 %collective-permute-start.31 = (bf16[128,512]{1,0:T(8,128)(2,1)S(1)}, bf16[128,512]{1,0:T(8,128)(2,1)S(1)}, u32[]{:S(2)}, u32[]{:S(2)}) collective-permute-start(bf16[128,512]{1,0:T(8,128)(2,1)S(1)} %slice.251), channel_id=1, source_target_pairs={{0,8},{4,12},{8,16},{12,20},{16,24},{20,28},{24,0},{28,4},{1,9},{5... | collective-permute-start | bytes 393224 | tf_op jit(solution)/shard_map/ppermute | solution.py:182
  126.6 15.0 %collective-permute-start.24 = (bf16[128,512]{1,0:T(8,128)(2,1)S(1)}, bf16[128,512]{1,0:T(8,128)(2,1)S(1)}, u32[]{:S(2)}, u32[]{:S(2)}) collective-permute-start(bf16[128,512]{1,0:T(8,128)(2,1)S(1)} %slice.252), channel_id=1, source_target_pairs={{0,8},{4,12},{8,16},{12,20},{16,24},{20,28},{24,0},{28,4},{1,9},{5... | collective-permute-start | bytes 393224 | tf_op jit(solution)/shard_map/ppermute | solution.py:182
  138.8 11.2 %collective-permute-start.32 = (bf16[128,512]{1,0:T(8,128)(2,1)S(1)}, bf16[128,512]{1,0:T(8,128)(2,1)S(1)}, u32[]{:S(2)}, u32[]{:S(2)}) collective-permute-start(bf16[128,512]{1,0:T(8,128)(2,1)S(1)} %fusion.38), channel_id=1, source_target_pairs={{0,8},{4,12},{8,16},{12,20},{16,24},{20,28},{24,0},{28,4},{1,9},{5... | collective-permute-start | bytes 393224 | tf_op jit(solution)/shard_map/ppermute | solution.py:182
  144.5 11.2 %collective-permute-start.44 = (bf16[128,512]{1,0:T(8,128)(2,1)S(1)}, bf16[128,512]{1,0:T(8,128)(2,1)S(1)}, u32[]{:S(2)}, u32[]{:S(2)}) collective-permute-start(bf16[128,512]{1,0:T(8,128)(2,1)S(1)} %fusion.33), channel_id=1, source_target_pairs={{0,8},{4,12},{8,16},{12,20},{16,24},{20,28},{24,0},{28,4},{1,9},{5... | collective-permute-start | bytes 393224 | tf_op jit(solution)/shard_map/ppermute | solution.py:182
  (33 other events, 281.8 us)

commit v2 on v1

--- a/solution.py
+++ b/solution.py
@@ -1,5 +1,7 @@
 import jax
 import jax.numpy as jnp
+from functools import partial
+
 from jax import lax
 from jax.experimental import pallas as pl
 from jax.experimental.pallas import tpu as pltpu
@@ -113,13 +115,15 @@
 CHUNKS = 4
 
 
-def copy_blocks(jobs, arrays, shapes, at=None):
-    def kernel(at_ref, *refs):
+def copy_blocks(jobs, arrays, shapes, me):
+    def kernel(me_ref, *refs):
         ins, outs, sem = refs[: len(arrays)], refs[len(arrays) : -1], refs[-1]
         copies = []
         for n, (source, row, rows, cols, target, to) in enumerate(jobs):
-            if row is None:
-                row = pl.multiple_of(at_ref[0], rows)
+            row, to = (
+                pl.multiple_of(place(me_ref[0]), rows) if callable(place) else place
+                for place in (row, to)
+            )
             copies.append(
                 pltpu.make_async_copy(
                     ins[source].at[pl.ds(row, rows), cols],
@@ -132,7 +136,6 @@
         for copy in copies:
             copy.wait()
 
-    at = jnp.zeros((1,), jnp.int32) if at is None else at
     moved = sum(s[0] * s[1] for s in shapes) * 2
     return pl.pallas_call(
         kernel,
@@ -141,9 +144,60 @@
         + [pl.BlockSpec(memory_space=pltpu.HBM)] * len(arrays),
         out_specs=[pl.BlockSpec(memory_space=pltpu.VMEM)] * len(shapes),
         scratch_shapes=[pltpu.SemaphoreType.DMA((len(jobs),))],
+        compiler_params=pltpu.CompilerParams(vmem_limit_bytes=24 * 1024 * 1024),
+        cost_estimate=pl.CostEstimate(flops=moved, bytes_accessed=2 * moved, transcendentals=0),
+    )(me, *arrays)
+
+
+def norm_kernel(tok_ref, gain_ref, out_ref):
+    def step(i, carry):
+        tile = pl.ds(pl.multiple_of(i * 16, 16), 16)
+        tok = tok_ref[tile].astype(jnp.float32)
+        factor = lax.rsqrt(jnp.mean(tok * tok, axis=-1, keepdims=True) + EPS)
+        out_ref[tile] = (tok * factor * gain_ref[...]).astype(jnp.bfloat16)
+        return carry
+
+    lax.fori_loop(0, tok_ref.shape[0] // 16, step, 0)
+
+
+def norm_rows(tokens, gain):
+    return pl.pallas_call(
+        norm_kernel,
+        out_shape=jax.ShapeDtypeStruct(tokens.shape, jnp.bfloat16),
         compiler_params=pltpu.CompilerParams(vmem_limit_bytes=8 * 1024 * 1024),
-        cost_estimate=pl.CostEstimate(flops=moved, bytes_accessed=2 * moved, transcendentals=0),
-    )(at, *arrays)
+        cost_estimate=pl.CostEstimate(
+            flops=8 * tokens.size, bytes_accessed=4 * tokens.size, transcendentals=0
+        ),
+    )(tokens, gain[None, :])
+
+
+def slot(core, k, e):
+    odd = (e // CORES) % 2
+    return 4 * core + (3, 2 * (1 - odd), 1, 2 * odd)[k]
+
+
+def block_row(core, k, rows, e):
+    return slot(core, k, e) * rows
+
+
+def row_scale(weights, me, ep):
+    count = len(weights)
+
+    def kernel(me_ref, *refs):
+        for c in range(CORES):
+            for k in range(count):
+                row = pl.ds(c * ep + me_ref[0], 1)
+                refs[-1][pl.ds(slot(c, k, me_ref[0]), 1)] = refs[k][row]
+
+    shape = (CORES * count, weights[0].shape[1])
+    vmem = pl.BlockSpec(memory_space=pltpu.VMEM)
+    return pl.pallas_call(
+        kernel,
+        out_shape=jax.ShapeDtypeStruct(shape, jnp.float32),
+        in_specs=[pl.BlockSpec(memory_space=pltpu.SMEM)] + [vmem] * count,
+        out_specs=vmem,
+        compiler_params=pltpu.CompilerParams(vmem_limit_bytes=4 * 1024 * 1024),
+    )(me, *weights)
 
 
 def column_body(
@@ -159,12 +213,11 @@
     shared_down,
 ):
     ep, tp = lax.axis_size("ep"), lax.axis_size("tp")
-    levels = ep // CORES
-    me = lax.axis_index("ep")
+    me = lax.axis_index("ep").astype(jnp.int32)[None]
     tok_rows, features = tokens.shape
 
     z_up = [(i, (i + CORES) % ep) for i in range(ep)]
-    swap = [(i, i ^ 1) for i in range(ep)]
+    swap, near_z, far_z = ([(i, i ^ step) for i in range(ep)] for step in (1, 2, 4))
     x_swap = [(i, i ^ 1) for i in range(tp)]
     y_swap = [(i, i ^ 2) for i in range(tp)]
     both_swap = [(i, i ^ 3) for i in range(tp)]
@@ -180,6 +233,12 @@
 
     def up(a):
         return lax.ppermute(a, "ep", z_up)
+
+    def to_near(a):
+        return lax.ppermute(a, "ep", near_z)
+
+    def to_far(a):
+        return lax.ppermute(a, "ep", far_z)
 
     def other_core(a):
         return lax.ppermute(a, "ep", swap)
@@ -188,10 +247,10 @@
     features = tokens.shape[1]
     every = slice(0, features)
     shared = copy_blocks(
-        [(i, None, s, every, 0, i * s) for i in range(3)],
+        [(i, lambda e: e * s, s, every, 0, i * s) for i in range(3)],
         (shared_gate, shared_up, shared_down),
         [(3 * s, features)],
-        at=(me * s).astype(jnp.int32)[None],
+        me,
     )[0]
     gate, upw, down = expert_gate[0], expert_up[0], expert_down[0]
 
@@ -203,33 +262,25 @@
 
     gx, gy = over_x(gate), over_y(gate)
     ux, uy = over_x(upw), over_y(upw)
-    sx, sy, sd = over_x(shared), over_y(shared), across(shared)
-    gd, ud = over_y(gx), over_x(uy)
-
-    own_blocks, other_blocks = [tokens], [other_core(tokens)]
-    weights = [jnp.concatenate([dense, other_core(dense)], axis=0)]
-    for _ in range(1, levels):
-        own_blocks.append(up(own_blocks[-1]))
-        other_blocks.append(other_core(own_blocks[-1]))
-        weights.append(up(weights[-1]))
+    sx, sy = over_x(shared), over_y(shared)
+    gd, ud, sd = over_y(gx), over_x(uy), over_x(sy)
+
+    normed = norm_rows(tokens, norm_gain)
+    a1 = to_far(normed)
+    own_blocks = [normed, to_near(normed), a1, to_near(a1)]
+    other_blocks = [other_core(block) for block in own_blocks]
+    pair = jnp.concatenate([dense, other_core(dense)], axis=0)
+    w1 = to_far(pair)
+    weights = [pair, to_near(pair), w1, to_near(w1)]
 
     quarter = features // CHUNKS
     down_rows = []
-    for n, (lo, hi) in enumerate(((0, 1), (1, 2), (2, 4))):
+    for n, (lo, hi) in enumerate(((0, 1), (1, 2), (2, 3), (3, 4))):
         piece = down[:, lo * quarter : hi * quarter]
         dx, dy = over_x(piece), over_y(piece)
         dd = across(piece)
         down_rows.append((piece, dx, dy, dd))
 
-    def normed_of(part):
-        tok = part.astype(jnp.float32)
-        factor = lax.rsqrt(jnp.mean(tok * tok, axis=-1, keepdims=True) + EPS)
-        return (tok * factor * norm_gain).astype(jnp.bfloat16)
-
-    def joined(pieces):
-        return jnp.concatenate(pieces, axis=0)
-
-    order = list(range(1, levels)) + [0]
     shares = (shared, sx, sy, sd)
     n = gate.shape[0]
     units = 4 * n + 4 * s
@@ -237,40 +288,50 @@
     arrays = (gate, gx, gy, gd, upw, ux, uy, ud, *shares)
     jobs = [(i, 0, n, every, i // 4, places[i % 4]) for i in range(8)]
     jobs += [(8 + i, t * s, s, every, t, 4 * n + i * s) for i in range(4) for t in range(2)]
-    g_all, u_all = copy_blocks(jobs, arrays, [(units, features)] * 2)
-    weights = lax.optimization_barrier((*weights, g_all))[:-1]
-
-    rows = joined(
-        [normed_of(own_blocks[r]) for r in order] + [normed_of(other_blocks[r]) for r in order]
-    )
-    picked = [lax.dynamic_slice_in_dim(weights[r].reshape(2, ep, -1), me, 1, 1) for r in order]
-    scale = joined([p[c, 0] for c in range(2) for p in picked])[:, None]
+    blocks = (*own_blocks, *other_blocks)
+    jobs += [
+        (12 + 4 * c + k, 0, tok_rows, every, 2, partial(block_row, c, k, tok_rows))
+        for c in range(CORES)
+        for k in range(4)
+    ]
+    shapes = [(units, features)] * 2 + [(8 * tok_rows, features)]
+    g_all, u_all, rows = copy_blocks(jobs, (*arrays, *blocks), shapes, me)
+    weights = lax.optimization_barrier((*weights, own_blocks[3]))[:-1]
+    scale = row_scale(weights, me, ep).reshape(-1, 1)
     routed = (jnp.arange(units) < 4 * n)[None, :]
     value = jax.nn.silu(against(rows, g_all)) * against(rows, u_all)
     hidden = (value * jnp.where(routed, scale, 1.0)).astype(jnp.bfloat16)
 
-    own_rows = levels * tok_rows
-
-    def product(c, lo, hi):
-        arrays = (*down_rows[c], *shares)
-        jobs = [(i, 0, n, slice(0, hi - lo), 0, i * n) for i in range(4)]
-        jobs += [(4 + i, 2 * s, s, slice(lo, hi), 0, 4 * n + i * s) for i in range(4)]
-        down_all = copy_blocks(jobs, arrays, [(units, hi - lo)])[0]
-        part = jnp.dot(hidden, down_all, preferred_element_type=jnp.float32)
-        return with_layout_constraint(part, Layout(major_to_minor=(0, 1)))
-
-    parts = [product(0, 0, quarter), product(1, quarter, 2 * quarter)]
-    wide = product(2, 2 * quarter, features)
-    parts += [wide[:, :quarter], wide[:, quarter:]]
-    outs = []
+    own_rows = 4 * tok_rows
+
+    parts = []
+    for pieces in down_rows:
+        jobs, count = [], pieces[0].shape[1] // quarter
+        for t in range(count):
+            cols = slice(t * quarter, (t + 1) * quarter)
+            jobs += [(i, 0, n, cols, t, i * n) for i in range(4)]
+            at = (len(parts) + t) * quarter
+            cols = slice(at, at + quarter)
+            jobs += [(4 + i, 2 * s, s, cols, t, 4 * n + i * s) for i in range(4)]
+        downs = copy_blocks(jobs, (*pieces, *shares), [(units, quarter)] * count, me)
+        for rows_down in downs:
+            part = jnp.dot(hidden, rows_down, preferred_element_type=jnp.float32)
+            parts.append(with_layout_constraint(part, Layout(major_to_minor=(0, 1))))
+    mine, arrived = [], []
     for part in parts:
         swapped = other_core(part[own_rows:].astype(jnp.bfloat16))
-        total = part[:own_rows] + swapped.astype(jnp.float32)
-        moving = total[:tok_rows]
-        for r in range(1, levels):
-            arrived = up(moving.astype(jnp.bfloat16))
-            moving = total[r * tok_rows : (r + 1) * tok_rows] + arrived.astype(jnp.float32)
-        outs.append(moving.astype(jnp.bfloat16))
+        for r in range(1, 4):
+            block = part[(r - 1) * tok_rows : r * tok_rows]
+            moving = block + swapped[(r - 1) * tok_rows : r * tok_rows].astype(jnp.float32)
+            if r > 1:
+                moving = moving + came.astype(jnp.float32)
+            moving = moving.astype(jnp.bfloat16)
+            came = up(moving)
+        moving = part[3 * tok_rows : own_rows] + swapped[3 * tok_rows :].astype(jnp.float32)
+        mine.append(moving)
+        arrived.append(came)
+    arrived = lax.optimization_barrier(tuple(arrived))
+    outs = [(a + b).astype(jnp.bfloat16) for a, b in zip(mine, arrived)]
     return jnp.concatenate(outs, axis=1)
 
 

time: 165 us -> 144 us (0.87)
  waiting for transfers between devices: 94.1 us -> 65.7 us
  other arithmetic: 9.84 us -> 1.6 us
  starting transfers between devices: 37.2 us -> 44 us
  local copies, waits for them, and re-layouts: 9.23 us -> 15.9 us
  Pallas kernels: 3.87 us -> 6.33 us
    ppermute x18 -> x12, waiting for transfers between devices: 61 us -> 32.2 us  [up(): return lax.ppermute(a, 'ep', z_up)]
    ppermute x0 -> x6, starting transfers between devices: none -> 10.4 us  [the longest x4 5.18 us: to_near(): return lax.ppermute(a, 'ep', near_z)]
    ppermute x7 -> x8, waiting for transfers between devices: 8.64 us -> 17.2 us  [over_y(): return lax.ppermute(a, 'tp', y_swap)]
    ppermute x7 -> x9, waiting for transfers between devices: 13.3 us -> 4.94 us  [over_x(): return lax.ppermute(a, 'tp', x_swap)]
    unnamed x31 -> x62, local copies, waits for them, and re-layouts: 6.36 us -> 13 us
    ppermute x0 -> x6, waiting for transfers between devices: none -> 6.12 us  [the longest x4 4.15 us: to_near(): return lax.ppermute(a, 'ep', near_z)]
    ppermute x4, starting transfers between devices: 8.13 us -> 2.32 us  [across(): return lax.ppermute(a, 'tp', both_swap)]
    ppermute x4, waiting for transfers between devices: 10.8 us -> 5.27 us  [across(): return lax.ppermute(a, 'tp', both_swap)]
  transfers between devices with their start and end apart: 45 -> 48, of which waited for: 23 -> 23; matrix products, arithmetic and copies ran while one was open for 7% -> 3% of each run, Pallas kernels for 2% -> 3%
where the time goes in v2:
time: 144 us
  waiting for transfers between devices  65.7 us (46%)
  starting transfers between devices  44 us (31%)
  local copies, waits for them, and re-layouts  15.9 us (11%)
  matrix products  9.79 us (7%)
  Pallas kernels  6.33 us (4%)
  other arithmetic  1.6 us (1%)
    ppermute x12, waiting for transfers between devices, up(): return lax.ppermute(a, 'ep', z_up)  32.2 us
    ppermute x8, waiting for transfers between devices, over_y(): return lax.ppermute(a, 'tp', y_swap)  17.2 us
    ppermute x9, starting transfers between devices, over_x(): return lax.ppermute(a, 'tp', x_swap)  13.3 us
    unnamed x62, local copies, waits for them, and re-layouts  13 us
    ppermute x8, starting transfers between devices, over_y(): return lax.ppermute(a, 'tp', y_swap)  10 us
    dot_general x2, matrix products, against(): lax.dot_general(rows, weight, (((1,), (1,)), ((), ())), preferred_element...  5.68 us
    ppermute x12, starting transfers between devices, up(): return lax.ppermute(a, 'ep', z_up)  5.63 us
    pallas_call x6, Pallas kernels, copy_blocks(): pl.pallas_call(kernel, out_shape=[jax.ShapeDtypeStruct(s, jnp.bfloat16) f...  5.4 us
  transfers between devices with their start and end apart: 48, of which 23 were waited for; matrix products, arithmetic and copies ran while one was open for 3% of the time, Pallas kernels for 3%

profile of v2, /device:TPU:0, one launch (start us, length us, event | category | flops | bytes accessed | tf_op | source)
XLA Modules:
  0.0 143.8 jit_solution(11419819877850462043)
XLA Ops:
  3.3 2.6 %collective-permute-start.41 = (bf16[128,512]{1,0:T(8,128)(2,1)S(1)}, bf16[128,512]{1,0:T(8,128)(2,1)S(1)}, u32[]{:S(2)}, u32[]{:S(2)}) collective-permute-start(bf16[128,512]{1,0:T(8,128)(2,1)S(1)} %get-tuple-element.28.refs_0_), channel_id=1, source_target_pairs={{0,1},{1,0},{2,3},{3,2},{4,5},{5,4},{6,7},{7,6},{8,9},{9,8},{10,11... | collective-permute-start | bytes 393224 | tf_op jit(solution)/shard_map/ppermute | solution.py:226
  9.3 2.6 %collective-permute-start.18 = (f32[16,128]{1,0:T(8,128)S(1)}, f32[16,128]{1,0:T(8,128)S(1)}, u32[]{:S(2)}, u32[]{:S(2)}) collective-permute-start(f32[16,128]{1,0:T(8,128)S(1)} %pad_maximum_fusion.1.refs_0_), channel_id=1, source_target_pairs={{0,16},{4,20},{8,24},{12,28},{16,0},{20,4},{24,8},{28,12},{1,17},{... | collective-permute-start | bytes 24584 | tf_op jit(solution)/shard_map/ppermute | solution.py:241
  15.4 2.1 %collective-permute-done.17.refs_1_ = f32[16,128]{1,0:T(8,128)S(1)} collective-permute-done((f32[16,128]{1,0:T(8,128)S(1)}, f32[16,128]{1,0:T(8,128)S(1)}, u32[]{:S(2)}, u32[]{:S(2)}) %collective-permute-start.17) | collective-permute-done | bytes 8224 | tf_op jit(solution)/shard_map/ppermute | solution.py:238
  19.7 2.1 %collective-permute-done.19.refs_3_ = f32[16,128]{1,0:T(8,128)S(1)} collective-permute-done((f32[16,128]{1,0:T(8,128)S(1)}, f32[16,128]{1,0:T(8,128)S(1)}, u32[]{:S(2)}, u32[]{:S(2)}) %collective-permute-start.19) | collective-permute-done | bytes 8224 | tf_op jit(solution)/shard_map/ppermute | solution.py:238
  33.4 2.6 %collective-permute-start.10 = (bf16[128,2048]{1,0:T(8,128)(2,1)S(1)}, bf16[128,2048]{1,0:T(8,128)(2,1)S(1)}, u32[]{:S(2)}, u32[]{:S(2)}) collective-permute-start(bf16[128,2048]{1,0:T(8,128)(2,1)S(1)} %shard_map.101.refs_12_), channel_id=1, source_target_pairs={{0,16},{4,20},{8,24},{12,28},{16,0},{20,4},{24,8},{28,12},{1,17},{... | collective-permute-start | bytes 1572872 | tf_op jit(solution)/shard_map/ppermute | solution.py:241
  48.4 5.3 %collective-permute-done.22.refs_3_ = bf16[128,512]{1,0:T(8,128)(2,1)S(1)} collective-permute-done((bf16[128,512]{1,0:T(8,128)(2,1)S(1)}, bf16[128,512]{1,0:T(8,128)(2,1)S(1)}, u32[]{:S(2)}, u32[]{:S(2)}) %collective-permute-start.22) | collective-permute-done | bytes 131104 | tf_op jit(solution)/shard_map/ppermute | solution.py:232
  55.7 3.6 %collective-permute-done.6.refs_9_.refs_5_ = bf16[48,2048]{1,0:T(8,128)(2,1)S(1)} collective-permute-done((bf16[48,2048]{1,0:T(8,128)(2,1)S(1)}, bf16[48,2048]{1,0:T(8,128)(2,1)S(1)}, u32[]{:S(2)}, u32[]{:S(2)}) %collective-permute-start.6) | collective-permute-done | bytes 196640 | tf_op jit(solution)/shard_map/ppermute | solution.py:226
  64.5 8.0 %collective-permute-done.4.refs_6_ = bf16[128,2048]{1,0:T(8,128)(2,1)S(1)} collective-permute-done((bf16[128,2048]{1,0:T(8,128)(2,1)S(1)}, bf16[128,2048]{1,0:T(8,128)(2,1)S(1)}, u32[]{:S(2)}, u32[]{:S(2)}) %collective-permute-start.4) | collective-permute-done | bytes 524320 | tf_op jit(solution)/shard_map/ppermute | solution.py:229
  73.0 8.0 %collective-permute-done.1.refs_2_ = bf16[128,2048]{1,0:T(8,128)(2,1)S(1)} collective-permute-done((bf16[128,2048]{1,0:T(8,128)(2,1)S(1)}, bf16[128,2048]{1,0:T(8,128)(2,1)S(1)}, u32[]{:S(2)}, u32[]{:S(2)}) %collective-permute-start.1) | collective-permute-done | bytes 524320 | tf_op jit(solution)/shard_map/ppermute | solution.py:229
  92.8 2.6 %fusion.29 = f32[1024,576]{0,1:T(8,128)S(1)} fusion(bf16[1024,2048]{1,0:T(8,128)(2,1)S(1)} %get-tuple-element.16, bf16[576,2048]{1,0:T(8,128)(2,1)S(1)} %get-tuple-element.17), kind=kOutput, calls=%fused_computation.60 | convolution fusion | flops 2415919104 | bytes 8912896 | tf_op jit(solution)/shard_map/dot_general | solution.py:19
  95.5 3.0 %multiply_convert_fusion = bf16[1024,576]{0,1:T(8,128)(2,1)S(1)} fusion(f32[1024,576]{0,1:T(8,128)S(1)} %fusion.29, f32[1024]{0:T(1024)S(1)} %bitcast.33, pred[576]{0:T(1024)(128)(4,1)S(1)} %iota_compare_fusion.2, bf16[1024,2048]{1,0:T(8,128)(2,1)S(1)} %get-tuple-element.16, bf16[576,2048]{1,0:T(8,128)(2,1)S(1)} %get-tuple-element.18), kind=kOutput, calls=%fused_computation | convolution fusion | flops 2420637696 | bytes 10097216 | tf_op jit(solution)/shard_map/dot_general | solution.py:19
  106.6 2.9 %collective-permute-start.24 = (bf16[128,512]{1,0:T(8,128)(2,1)S(1)}, bf16[128,512]{1,0:T(8,128)(2,1)S(1)}, u32[]{:S(2)}, u32[]{:S(2)}) collective-permute-start(bf16[128,512]{1,0:T(8,128)(2,1)S(1)} %fusion.21), channel_id=1, source_target_pairs={{0,8},{4,12},{8,16},{12,20},{16,24},{20,28},{24,0},{28,4},{1,9},{5... | collective-permute-start | bytes 393224 | tf_op jit(solution)/shard_map/ppermute | solution.py:235
  109.6 2.9 %collective-permute-done.45 = bf16[128,512]{1,0:T(8,128)(2,1)S(1)} collective-permute-done((bf16[128,512]{1,0:T(8,128)(2,1)S(1)}, bf16[128,512]{1,0:T(8,128)(2,1)S(1)}, u32[]{:S(2)}, u32[]{:S(2)}) %collective-permute-start.45) | collective-permute-done | bytes 131104 | tf_op jit(solution)/shard_map/ppermute | solution.py:235
  112.6 2.7 %collective-permute-done.38 = bf16[128,512]{1,0:T(8,128)(2,1)S(1)} collective-permute-done((bf16[128,512]{1,0:T(8,128)(2,1)S(1)}, bf16[128,512]{1,0:T(8,128)(2,1)S(1)}, u32[]{:S(2)}, u32[]{:S(2)}) %collective-permute-start.38) | collective-permute-done | bytes 131104 | tf_op jit(solution)/shard_map/ppermute | solution.py:235
  115.4 2.7 %collective-permute-done.31 = bf16[128,512]{1,0:T(8,128)(2,1)S(1)} collective-permute-done((bf16[128,512]{1,0:T(8,128)(2,1)S(1)}, bf16[128,512]{1,0:T(8,128)(2,1)S(1)}, u32[]{:S(2)}, u32[]{:S(2)}) %collective-permute-start.31) | collective-permute-done | bytes 131104 | tf_op jit(solution)/shard_map/ppermute | solution.py:235
  118.2 2.7 %collective-permute-done.24 = bf16[128,512]{1,0:T(8,128)(2,1)S(1)} collective-permute-done((bf16[128,512]{1,0:T(8,128)(2,1)S(1)}, bf16[128,512]{1,0:T(8,128)(2,1)S(1)}, u32[]{:S(2)}, u32[]{:S(2)}) %collective-permute-start.24) | collective-permute-done | bytes 131104 | tf_op jit(solution)/shard_map/ppermute | solution.py:235
  121.0 2.7 %collective-permute-done.46 = bf16[128,512]{1,0:T(8,128)(2,1)S(1)} collective-permute-done((bf16[128,512]{1,0:T(8,128)(2,1)S(1)}, bf16[128,512]{1,0:T(8,128)(2,1)S(1)}, u32[]{:S(2)}, u32[]{:S(2)}) %collective-permute-start.46) | collective-permute-done | bytes 131104 | tf_op jit(solution)/shard_map/ppermute | solution.py:235
  123.9 2.7 %collective-permute-done.39 = bf16[128,512]{1,0:T(8,128)(2,1)S(1)} collective-permute-done((bf16[128,512]{1,0:T(8,128)(2,1)S(1)}, bf16[128,512]{1,0:T(8,128)(2,1)S(1)}, u32[]{:S(2)}, u32[]{:S(2)}) %collective-permute-start.39) | collective-permute-done | bytes 131104 | tf_op jit(solution)/shard_map/ppermute | solution.py:235
  126.7 2.7 %collective-permute-done.32 = bf16[128,512]{1,0:T(8,128)(2,1)S(1)} collective-permute-done((bf16[128,512]{1,0:T(8,128)(2,1)S(1)}, bf16[128,512]{1,0:T(8,128)(2,1)S(1)}, u32[]{:S(2)}, u32[]{:S(2)}) %collective-permute-start.32) | collective-permute-done | bytes 131104 | tf_op jit(solution)/shard_map/ppermute | solution.py:235
  129.5 2.7 %collective-permute-done.25 = bf16[128,512]{1,0:T(8,128)(2,1)S(1)} collective-permute-done((bf16[128,512]{1,0:T(8,128)(2,1)S(1)}, bf16[128,512]{1,0:T(8,128)(2,1)S(1)}, u32[]{:S(2)}, u32[]{:S(2)}) %collective-permute-start.25) | collective-permute-done | bytes 131104 | tf_op jit(solution)/shard_map/ppermute | solution.py:235
  132.3 2.7 %collective-permute-done.47 = bf16[128,512]{1,0:T(8,128)(2,1)S(1)} collective-permute-done((bf16[128,512]{1,0:T(8,128)(2,1)S(1)}, bf16[128,512]{1,0:T(8,128)(2,1)S(1)}, u32[]{:S(2)}, u32[]{:S(2)}) %collective-permute-start.47) | collective-permute-done | bytes 131104 | tf_op jit(solution)/shard_map/ppermute | solution.py:235
  135.0 2.8 %collective-permute-done.40 = bf16[128,512]{1,0:T(8,128)(2,1)S(1)} collective-permute-done((bf16[128,512]{1,0:T(8,128)(2,1)S(1)}, bf16[128,512]{1,0:T(8,128)(2,1)S(1)}, u32[]{:S(2)}, u32[]{:S(2)}) %collective-permute-start.40) | collective-permute-done | bytes 131104 | tf_op jit(solution)/shard_map/ppermute | solution.py:235
  137.8 2.8 %collective-permute-done.33 = bf16[128,512]{1,0:T(8,128)(2,1)S(1)} collective-permute-done((bf16[128,512]{1,0:T(8,128)(2,1)S(1)}, bf16[128,512]{1,0:T(8,128)(2,1)S(1)}, u32[]{:S(2)}, u32[]{:S(2)}) %collective-permute-start.33) | collective-permute-done | bytes 131104 | tf_op jit(solution)/shard_map/ppermute | solution.py:235
  140.6 2.1 %collective-permute-done.26 = bf16[128,512]{1,0:T(8,128)(2,1)S(1)} collective-permute-done((bf16[128,512]{1,0:T(8,128)(2,1)S(1)}, bf16[128,512]{1,0:T(8,128)(2,1)S(1)}, u32[]{:S(2)}, u32[]{:S(2)}) %collective-permute-start.26) | collective-permute-done | bytes 131104 | tf_op jit(solution)/shard_map/ppermute | solution.py:235
  (173 shorter events, 65.7 us)
Async XLA Ops:
  3.3 20.6 %collective-permute-start.41 = (bf16[128,512]{1,0:T(8,128)(2,1)S(1)}, bf16[128,512]{1,0:T(8,128)(2,1)S(1)}, u32[]{:S(2)}, u32[]{:S(2)}) collective-permute-start(bf16[128,512]{1,0:T(8,128)(2,1)S(1)} %get-tuple-element.28.refs_0_), channel_id=1, source_target_pairs={{0,1},{1,0},{2,3},{3,2},{4,5},{5,4},{6,7},{7,6},{8,9},{9,8},{10,11... | collective-permute-start | bytes 393224 | tf_op jit(solution)/shard_map/ppermute | solution.py:226
  5.8 18.2 %collective-permute-start.42 = (bf16[128,512]{1,0:T(8,128)(2,1)S(1)}, bf16[128,512]{1,0:T(8,128)(2,1)S(1)}, u32[]{:S(2)}, u32[]{:S(2)}) collective-permute-start(bf16[128,512]{1,0:T(8,128)(2,1)S(1)} %get-tuple-element.28.refs_0_), channel_id=1, source_target_pairs={{0,2},{1,3},{2,0},{3,1},{4,6},{5,7},{6,4},{7,5},{8,10},{9,11},{10,... | collective-permute-start | bytes 393224 | tf_op jit(solution)/shard_map/ppermute | solution.py:229
  7.3 18.5 %collective-permute-start.43 = (bf16[128,512]{1,0:T(8,128)(2,1)S(1)}, bf16[128,512]{1,0:T(8,128)(2,1)S(1)}, u32[]{:S(2)}, u32[]{:S(2)}) collective-permute-start(bf16[128,512]{1,0:T(8,128)(2,1)S(1)} %get-tuple-element.28.refs_0_), channel_id=1, source_target_pairs={{0,3},{1,2},{2,1},{3,0},{4,7},{5,6},{6,5},{7,4},{8,11},{9,10},{10,... | collective-permute-start | bytes 393224 | tf_op jit(solution)/shard_map/ppermute | solution.py:232
  7.4 20.0 %collective-permute-start.34 = (bf16[128,512]{1,0:T(8,128)(2,1)S(1)}, bf16[128,512]{1,0:T(8,128)(2,1)S(1)}, u32[]{:S(2)}, u32[]{:S(2)}) collective-permute-start(bf16[128,512]{1,0:T(8,128)(2,1)S(1)} %get-tuple-element.27.refs_0_), channel_id=1, source_target_pairs={{0,1},{1,0},{2,3},{3,2},{4,5},{5,4},{6,7},{7,6},{8,9},{9,8},{10,11... | collective-permute-start | bytes 393224 | tf_op jit(solution)/shard_map/ppermute | solution.py:226
  24.0 11.9 %collective-permute-start.27 = (bf16[128,512]{1,0:T(8,128)(2,1)S(1)}, bf16[128,512]{1,0:T(8,128)(2,1)S(1)}, u32[]{:S(2)}, u32[]{:S(2)}) collective-permute-start(bf16[128,512]{1,0:T(8,128)(2,1)S(1)} %get-tuple-element.29.refs_0_), channel_id=1, source_target_pairs={{0,1},{1,0},{2,3},{3,2},{4,5},{5,4},{6,7},{7,6},{8,9},{9,8},{10,11... | collective-permute-start | bytes 393224 | tf_op jit(solution)/shard_map/ppermute | solution.py:226
  25.9 12.3 %collective-permute-start.28 = (bf16[128,512]{1,0:T(8,128)(2,1)S(1)}, bf16[128,512]{1,0:T(8,128)(2,1)S(1)}, u32[]{:S(2)}, u32[]{:S(2)}) collective-permute-start(bf16[128,512]{1,0:T(8,128)(2,1)S(1)} %get-tuple-element.29.refs_0_), channel_id=1, source_target_pairs={{0,2},{1,3},{2,0},{3,1},{4,6},{5,7},{6,4},{7,5},{8,10},{9,11},{10,... | collective-permute-start | bytes 393224 | tf_op jit(solution)/shard_map/ppermute | solution.py:229
  27.4 12.1 %collective-permute-start.29 = (bf16[128,512]{1,0:T(8,128)(2,1)S(1)}, bf16[128,512]{1,0:T(8,128)(2,1)S(1)}, u32[]{:S(2)}, u32[]{:S(2)}) collective-permute-start(bf16[128,512]{1,0:T(8,128)(2,1)S(1)} %get-tuple-element.29.refs_0_), channel_id=1, source_target_pairs={{0,3},{1,2},{2,1},{3,0},{4,7},{5,6},{6,5},{7,4},{8,11},{9,10},{10,... | collective-permute-start | bytes 393224 | tf_op jit(solution)/shard_map/ppermute | solution.py:232
  31.3 13.7 %collective-permute-start.20 = (bf16[128,512]{1,0:T(8,128)(2,1)S(1)}, bf16[128,512]{1,0:T(8,128)(2,1)}, u32[]{:S(2)}, u32[]{:S(2)}) collective-permute-start(bf16[128,512]{1,0:T(8,128)(2,1)S(1)} %get-tuple-element.30.refs_0_), channel_id=1, source_target_pairs={{0,1},{1,0},{2,3},{3,2},{4,5},{5,4},{6,7},{7,6},{8,9},{9,8},{10,11... | collective-permute-start | bytes 393224 | tf_op jit(solution)/shard_map/ppermute | solution.py:226
  33.4 28.1 %collective-permute-start.10 = (bf16[128,2048]{1,0:T(8,128)(2,1)S(1)}, bf16[128,2048]{1,0:T(8,128)(2,1)S(1)}, u32[]{:S(2)}, u32[]{:S(2)}) collective-permute-start(bf16[128,2048]{1,0:T(8,128)(2,1)S(1)} %shard_map.101.refs_12_), channel_id=1, source_target_pairs={{0,16},{4,20},{8,24},{12,28},{16,0},{20,4},{24,8},{28,12},{1,17},{... | collective-permute-start | bytes 1572872 | tf_op jit(solution)/shard_map/ppermute | solution.py:241
  36.6 26.0 %collective-permute-start.9 = (bf16[128,2048]{1,0:T(8,128)(2,1)S(1)}, bf16[128,2048]{1,0:T(8,128)(2,1)S(1)}, u32[]{:S(2)}, u32[]{:S(2)}) collective-permute-start(bf16[128,2048]{1,0:T(8,128)(2,1)S(1)} %shard_map.101.refs_12_), channel_id=1, source_target_pairs={{0,8},{4,12},{8,0},{12,4},{16,24},{20,28},{24,16},{28,20},{1,9},{5... | collective-permute-start | bytes 1572872 | tf_op jit(solution)/shard_map/ppermute | solution.py:238
  38.8 25.2 %collective-permute-start = (bf16[128,2048]{1,0:T(8,128)(2,1)S(1)}, bf16[128,2048]{1,0:T(8,128)(2,1)S(1)}, u32[]{:S(2)}, u32[]{:S(2)}) collective-permute-start(bf16[128,2048]{1,0:T(8,128)(2,1)S(1)} %bitcast.26), channel_id=1, source_target_pairs={{0,1},{1,0},{2,3},{3,2},{4,5},{5,4},{6,7},{7,6},{8,9},{9,8},{10,11... | collective-permute-start | bytes 1572872 | tf_op jit(solution)/shard_map/ppermute | solution.py:226
  59.3 13.1 %collective-permute-start.4 = (bf16[128,2048]{1,0:T(8,128)(2,1)S(1)}, bf16[128,2048]{1,0:T(8,128)(2,1)S(1)}, u32[]{:S(2)}, u32[]{:S(2)}) collective-permute-start(bf16[128,2048]{1,0:T(8,128)(2,1)S(1)} %bitcast.29), channel_id=1, source_target_pairs={{0,2},{1,3},{2,0},{3,1},{4,6},{5,7},{6,4},{7,5},{8,10},{9,11},{10,... | collective-permute-start | bytes 1572872 | tf_op jit(solution)/shard_map/ppermute | solution.py:229
  61.5 19.6 %collective-permute-start.1 = (bf16[128,2048]{1,0:T(8,128)(2,1)S(1)}, bf16[128,2048]{1,0:T(8,128)(2,1)S(1)}, u32[]{:S(2)}, u32[]{:S(2)}) collective-permute-start(bf16[128,2048]{1,0:T(8,128)(2,1)S(1)} %bitcast.27), channel_id=1, source_target_pairs={{0,2},{1,3},{2,0},{3,1},{4,6},{5,7},{6,4},{7,5},{8,10},{9,11},{10,... | collective-permute-start | bytes 1572872 | tf_op jit(solution)/shard_map/ppermute | solution.py:229
  62.6 19.6 %collective-permute-start.3 = (bf16[128,2048]{1,0:T(8,128)(2,1)S(1)}, bf16[128,2048]{1,0:T(8,128)(2,1)S(1)}, u32[]{:S(2)}, u32[]{:S(2)}) collective-permute-start(bf16[128,2048]{1,0:T(8,128)(2,1)S(1)} %bitcast.30), channel_id=1, source_target_pairs={{0,1},{1,0},{2,3},{3,2},{4,5},{5,4},{6,7},{7,6},{8,9},{9,8},{10,11... | collective-permute-start | bytes 1572872 | tf_op jit(solution)/shard_map/ppermute | solution.py:226
  64.0 19.6 %collective-permute-start.11 = (bf16[128,2048]{1,0:T(8,128)(2,1)S(1)}, bf16[128,2048]{1,0:T(8,128)(2,1)S(1)}, u32[]{:S(2)}, u32[]{:S(2)}) collective-permute-start(bf16[128,2048]{1,0:T(8,128)(2,1)S(1)} %collective-permute-done.10.refs_14_), channel_id=1, source_target_pairs={{0,8},{4,12},{8,0},{12,4},{16,24},{20,28},{24,16},{28,20},{1,9},{5... | collective-permute-start | bytes 1572872 | tf_op jit(solution)/shard_map/ppermute | solution.py:238
  72.5 18.5 %collective-permute-start.14 = (bf16[128,2048]{1,0:T(8,128)(2,1)S(1)}, bf16[128,2048]{1,0:T(8,128)(2,1)S(1)}, u32[]{:S(2)}, u32[]{:S(2)}) collective-permute-start(bf16[128,2048]{1,0:T(8,128)(2,1)S(1)} %collective-permute-done.10.refs_14_), channel_id=1, source_target_pairs={{0,4},{4,0},{8,12},{12,8},{16,20},{20,16},{24,28},{28,24},{1,5},{5... | collective-permute-start | bytes 1572872 | tf_op jit(solution)/shard_map/ppermute | solution.py:244
  72.5 18.5 %collective-permute-start.13 = (bf16[128,2048]{1,0:T(8,128)(2,1)S(1)}, bf16[128,2048]{1,0:T(8,128)(2,1)S(1)}, u32[]{:S(2)}, u32[]{:S(2)}) collective-permute-start(bf16[128,2048]{1,0:T(8,128)(2,1)S(1)} %collective-permute-done.9.refs_13_), channel_id=1, source_target_pairs={{0,4},{4,0},{8,12},{12,8},{16,20},{20,16},{24,28},{28,24},{1,5},{5... | collective-permute-start | bytes 1572872 | tf_op jit(solution)/shard_map/ppermute | solution.py:244
  106.1 12.0 %collective-permute-start.31 = (bf16[128,512]{1,0:T(8,128)(2,1)S(1)}, bf16[128,512]{1,0:T(8,128)(2,1)S(1)}, u32[]{:S(2)}, u32[]{:S(2)}) collective-permute-start(bf16[128,512]{1,0:T(8,128)(2,1)S(1)} %fusion.16), channel_id=1, source_target_pairs={{0,8},{4,12},{8,16},{12,20},{16,24},{20,28},{24,0},{28,4},{1,9},{5... | collective-permute-start | bytes 393224 | tf_op jit(solution)/shard_map/ppermute | solution.py:235
  106.6 14.3 %collective-permute-start.24 = (bf16[128,512]{1,0:T(8,128)(2,1)S(1)}, bf16[128,512]{1,0:T(8,128)(2,1)S(1)}, u32[]{:S(2)}, u32[]{:S(2)}) collective-permute-start(bf16[128,512]{1,0:T(8,128)(2,1)S(1)} %fusion.21), channel_id=1, source_target_pairs={{0,8},{4,12},{8,16},{12,20},{16,24},{20,28},{24,0},{28,4},{1,9},{5... | collective-permute-start | bytes 393224 | tf_op jit(solution)/shard_map/ppermute | solution.py:235
  112.6 11.2 %collective-permute-start.46 = (bf16[128,512]{1,0:T(8,128)(2,1)S(1)}, bf16[128,512]{1,0:T(8,128)(2,1)S(1)}, u32[]{:S(2)}, u32[]{:S(2)}) collective-permute-start(bf16[128,512]{1,0:T(8,128)(2,1)S(1)} %fusion.8), channel_id=1, source_target_pairs={{0,8},{4,12},{8,16},{12,20},{16,24},{20,28},{24,0},{28,4},{1,9},{5... | collective-permute-start | bytes 393224 | tf_op jit(solution)/shard_map/ppermute | solution.py:235
  115.4 11.2 %collective-permute-start.39 = (bf16[128,512]{1,0:T(8,128)(2,1)S(1)}, bf16[128,512]{1,0:T(8,128)(2,1)S(1)}, u32[]{:S(2)}, u32[]{:S(2)}) collective-permute-start(bf16[128,512]{1,0:T(8,128)(2,1)S(1)} %fusion.13), channel_id=1, source_target_pairs={{0,8},{4,12},{8,16},{12,20},{16,24},{20,28},{24,0},{28,4},{1,9},{5... | collective-permute-start | bytes 393224 | tf_op jit(solution)/shard_map/ppermute | solution.py:235
  118.2 11.2 %collective-permute-start.32 = (bf16[128,512]{1,0:T(8,128)(2,1)S(1)}, bf16[128,512]{1,0:T(8,128)(2,1)S(1)}, u32[]{:S(2)}, u32[]{:S(2)}) collective-permute-start(bf16[128,512]{1,0:T(8,128)(2,1)S(1)} %fusion.18), channel_id=1, source_target_pairs={{0,8},{4,12},{8,16},{12,20},{16,24},{20,28},{24,0},{28,4},{1,9},{5... | collective-permute-start | bytes 393224 | tf_op jit(solution)/shard_map/ppermute | solution.py:235
  123.8 11.2 %collective-permute-start.47 = (bf16[128,512]{1,0:T(8,128)(2,1)S(1)}, bf16[128,512]{1,0:T(8,128)(2,1)S(1)}, u32[]{:S(2)}, u32[]{:S(2)}) collective-permute-start(bf16[128,512]{1,0:T(8,128)(2,1)S(1)} %fusion.10), channel_id=1, source_target_pairs={{0,8},{4,12},{8,16},{12,20},{16,24},{20,28},{24,0},{28,4},{1,9},{5... | collective-permute-start | bytes 393224 | tf_op jit(solution)/shard_map/ppermute | solution.py:235
  126.6 11.2 %collective-permute-start.40 = (bf16[128,512]{1,0:T(8,128)(2,1)S(1)}, bf16[128,512]{1,0:T(8,128)(2,1)S(1)}, u32[]{:S(2)}, u32[]{:S(2)}) collective-permute-start(bf16[128,512]{1,0:T(8,128)(2,1)S(1)} %fusion.15), channel_id=1, source_target_pairs={{0,8},{4,12},{8,16},{12,20},{16,24},{20,28},{24,0},{28,4},{1,9},{5... | collective-permute-start | bytes 393224 | tf_op jit(solution)/shard_map/ppermute | solution.py:235
  (55 other events, 616.6 us)
